TPU v7x, 512 devices: a 4x2x32 block of a 4x8x32 slice. The times are simulated.
512 devices in a mesh: grp: 2 (over y), sp: 64 (over z, core), tp: 4 (over x).
Axes of the slice: x: 4, y: 2, z: 32, core: 2. Of those that a mesh axis runs over, the one named last changes fastest.
The devices are a block of a 4x8x32 slice.
Arguments:
- tokens: bfloat16 [32768, 2048], P(('grp', 'sp'), 'tp'), parts along dimension 0, may hold values from -6 to 6
- norm_gain: float32 [2048], replicated, may hold values from 0.1 to 1.9
- ret_query_weight: bfloat16 [2048, 256], P('sp', 'tp'), may hold values from -0.125 to 0.125
- ret_key_weight: bfloat16 [2048, 256], P('sp', 'tp'), may hold values from -0.125 to 0.125
- ret_value_weight: bfloat16 [2048, 512], P('sp', 'tp'), may hold values from -0.125 to 0.125
- fox_query_weight: bfloat16 [2048, 512], P('sp', 'tp'), may hold values from -8 to 8
- fox_key_weight: bfloat16 [2048, 512], P('sp', 'tp'), may hold values from -0.125 to 0.125
- fox_value_weight: bfloat16 [2048, 512], P('sp', 'tp'), may hold values from -0.125 to 0.125
- ret_decay: float32 [8], P('tp'), may hold values from -1 to 0, as said below
- ret_state: float32 [16, 32, 64], P(('grp', 'tp')), parts along dimension 0, may hold values from -256 to 256
- head_norm_gain: float32 [512], P('tp'), may hold values from 0.1 to 1.9
- fox_gates: float32 [32768, 8], P('grp', 'tp'), parts along dimension 0, may hold values from -49152 to 0, as said below
- ret_out_weight: bfloat16 [512, 2048], P('tp', 'sp'), may hold values from -0.1875 to 0.1875
- fox_out_weight: bfloat16 [512, 2048], P('tp', 'sp'), may hold values from -1 to 1
Outputs:
- mixed: bfloat16 [32768, 2048], P(('grp', 'sp', 'tp')), parts along dimension 0
There are 2 independent parts, one for each index of `grp`. A program takes and returns all parts, laid end to end along the dimension named above; an argument that names none is the same for every part. Nothing has to cross between parts.
Inputs may be any that keep to these rules, and one draw needn't show every extreme that they name: `ret_decay`: each head's log decay is negative. `fox_gates`: along the positions each head's column never rises.
All inputs are finite; a program needn't handle non-finite values.
Results may differ from a plain program's by a relative error of at most 0.015.
The roundings to bfloat16 on the way count: a program that leaves them out, or rounds other values in their place, can miss the bound.
Values may be sent and summed in bfloat16 or wider, within the bound.
No kernel may reach another device: no remote copies, remote signals or barrier semaphores. Data moves between devices by JAX's collectives and lax.ppermute only.
A program may use at most 64 MiB of HBM per device.

v0:
```python
import jax
import jax.numpy as jnp
from jax import lax
from jax.sharding import Mesh
from jax.sharding import PartitionSpec as P

SP = ("sp_0", "sp_1")
GRP_SP = ("grp", "sp_0", "sp_1")
GRP_SP_TP = ("grp", "sp_0", "sp_1", "tp")


epsilon = 1e-06


def in_order(blocks, dim):
    shape = list(blocks.shape[1:])
    shape[dim] *= blocks.shape[0]
    return jnp.moveaxis(blocks, 0, dim).reshape(shape)


def from_everyone(array, axis):
    count = lax.axis_size(axis)
    return lax.all_to_all(
        jnp.broadcast_to(array[None], (count, *array.shape)), axis, 0, 0, tiled=True
    )


def collect_2(array, axis, dim):
    return in_order(from_everyone(array, axis), dim)


def sent_together(arrays, axis, dim, along):
    widths = [a.shape[along] for a in arrays]
    both = jnp.concatenate(arrays, axis=along)
    result = lax.all_gather(both, axis, axis=dim, tiled=True)
    return tuple(jnp.split(result, [sum(widths[:k]) for k in range(1, len(widths))], axis=along))


def all_blocks(array, axes, order):
    blocks = array
    for k in order:
        blocks = lax.all_gather(blocks, axes[k])
    done = order[::-1]
    back = [done.index(k) for k in range(len(axes))]
    blocks = blocks.transpose(*back, *range(len(axes), blocks.ndim))
    return blocks.reshape(-1, *array.shape)


def whole_of(array, axes, order, dim):
    return in_order(all_blocks(array, axes, order), dim)


def rows_first(arrays, axis, dims):
    turned = [jnp.moveaxis(a, dim, 0) for a, dim in zip(arrays, dims)]
    both = jnp.concatenate([t.reshape(len(t), -1) for t in turned], axis=1)
    result, at, gathered = (lax.all_gather(both, axis, axis=0, tiled=True), 0, [])
    for t, dim in zip(turned, dims):
        piece = result[:, at : at + t[0].size].reshape(-1, *t.shape[1:])
        gathered.append(jnp.moveaxis(piece, 0, dim))
        at += t[0].size
    return tuple(gathered)


def in_blocks(array, dim, count):
    before, after = (array.shape[:dim], array.shape[dim + 1 :])
    return jnp.moveaxis(array.reshape(*before, count, -1, *after), dim, 0)


def summed_on_arrival(array, axis, dim):
    blocks = in_blocks(array, dim, lax.axis_size(axis))
    arrived = lax.all_to_all(blocks, axis, split_axis=0, concat_axis=0, tiled=True)
    return arrived.astype(jnp.float32).sum(axis=0)


def head_group_norm(joined_output, norm_gains):
    center = joined_output - jnp.mean(joined_output, axis=-1, keepdims=True)
    spread = jnp.mean(center * center, axis=-1, keepdims=True)
    normal = (
        center
        * lax.rsqrt(spread + epsilon)
        * norm_gains.reshape(joined_output.shape[1], joined_output.shape[2])
    )
    return normal.reshape(joined_output.shape[0], -1).astype(jnp.bfloat16)


def softmax_update(
    current,
    query_heads,
    query_gates,
    query_pos,
    key_block,
    value_block,
    gate_block,
    key_pos,
    score_scale,
):
    top_now, total_now, weighted = current
    logits = (
        jnp.einsum("qhd,khd->hqk", query_heads, key_block, preferred_element_type=jnp.float32)
        * score_scale
    )
    logits = logits + query_gates[:, :, None] - gate_block[:, None, :]
    logits = jnp.where(key_pos[None, None, :] <= query_pos[None, :, None], logits, -jnp.inf)
    top_new = jnp.maximum(top_now, jnp.max(logits, axis=-1))
    weights_new = jnp.exp(logits - top_new[:, :, None])
    rescale = jnp.exp(top_now - top_new)
    total_new = total_now * rescale + jnp.sum(weights_new, axis=-1)
    weighted_new = weighted * rescale[:, :, None] + jnp.einsum(
        "hqk,khd->hqd",
        weights_new.astype(jnp.bfloat16),
        value_block,
        preferred_element_type=jnp.float32,
    )
    return (top_new, total_new, weighted_new)


def local(
    tokens,
    norm_gain,
    ret_query_weight,
    ret_key_weight,
    ret_value_weight,
    fox_query_weight,
    fox_key_weight,
    fox_value_weight,
    ret_decay,
    ret_state,
    head_norm_gain,
    fox_gates,
    ret_out_weight,
    fox_out_weight,
):
    sequence_length = tokens.shape[0]
    gathered = collect_2(tokens, "tp", 1)
    widened = gathered.astype(jnp.float32)
    normed = (
        widened
        * lax.rsqrt(jnp.mean(widened * widened, axis=-1, keepdims=True) + epsilon)
        * norm_gain
    ).astype(jnp.bfloat16)
    portions = sent_together(
        (
            ret_query_weight,
            ret_key_weight,
            ret_value_weight,
            fox_query_weight,
            fox_key_weight,
            fox_value_weight,
        ),
        SP,
        0,
        1,
    )
    sums = tuple(
        (jnp.dot(normed, portion, preferred_element_type=jnp.float32) for portion in portions)
    )
    ret_query, ret_key, ret_value, fox_query, fox_key, fox_value = [
        result.astype(jnp.bfloat16) for result in sums
    ]
    ret_heads = ret_decay.shape[0]
    key_size = ret_query.shape[1] // ret_heads
    value_size = ret_value.shape[1] // ret_heads
    place = lax.axis_index(SP)
    offset = place * sequence_length
    queries = ret_query.astype(jnp.float32).reshape(sequence_length, ret_heads, key_size)
    keys_local = ret_key.astype(jnp.float32).reshape(
        sequence_length, ret_heads, key_size
    ) * key_size ** (-0.5)
    values_local = ret_value.astype(jnp.float32).reshape(sequence_length, ret_heads, value_size)
    positions = jnp.arange(sequence_length, dtype=jnp.float32)
    spread = positions[:, None] - positions[None, :]
    within = jnp.where(
        spread[None] >= 0, jnp.exp(jnp.maximum(spread, 0.0)[None] * ret_decay[:, None, None]), 0.0
    )
    leading = jnp.exp((positions + 1.0)[:, None] * ret_decay[None, :])
    trailing = jnp.exp((sequence_length - 1.0 - positions)[:, None] * ret_decay[None, :])
    scores = jnp.einsum("ihd,jhd->hij", queries, keys_local) * within
    inner_value = jnp.einsum("hij,jhe->ihe", scores, values_local)
    summary = jnp.einsum("jhd,jhe->hde", keys_local * trailing[:, :, None], values_local)
    portion = whole_of(summary[None], SP, (0, 1), 0)
    shard_ids = jnp.arange(portion.shape[0], dtype=jnp.int32)
    distance = jnp.maximum(place - shard_ids - 1, 0).astype(jnp.float32) * sequence_length
    weight = jnp.where(
        (shard_ids < place)[:, None], jnp.exp(distance[:, None] * ret_decay[None, :]), 0.0
    )
    before = jnp.einsum("sh,shde->hde", weight, portion)
    entering = jnp.exp(offset.astype(jnp.float32) * ret_decay)[:, None, None] * ret_state + before
    carried_state = jnp.einsum("ihd,hde->ihe", queries, entering) * leading[:, :, None]
    retention_mixed = head_group_norm(inner_value + carried_state, head_norm_gain)
    fox_heads = fox_gates.shape[1]
    head_size = fox_query.shape[1] // fox_heads
    score_scale = head_size ** (-0.5)
    starting = (
        jnp.full((fox_heads, sequence_length), -1e30, jnp.float32),
        jnp.zeros((fox_heads, sequence_length), jnp.float32),
        jnp.zeros((fox_heads, sequence_length, head_size), jnp.float32),
    )
    query_heads = fox_query.reshape(sequence_length, fox_heads, head_size)
    own_gates = lax.dynamic_slice_in_dim(fox_gates, offset, sequence_length, 0).T
    query_pos = offset + jnp.arange(sequence_length, dtype=jnp.int32)
    last_query = offset + sequence_length - 1

    def attend(running, portion, first_key):
        key_rows, value_rows = portion
        count = key_rows.shape[0]
        block_rows = next(
            (candidate for candidate in (2048, 1024, 512) if count % candidate == 0), count
        )

        def advance(state_now, number):
            key_start = first_key + number * block_rows

            def compute(current):
                key_block = lax.dynamic_slice_in_dim(
                    key_rows, number * block_rows, block_rows, 0
                ).reshape(block_rows, fox_heads, head_size)
                value_block = lax.dynamic_slice_in_dim(
                    value_rows, number * block_rows, block_rows, 0
                ).reshape(block_rows, fox_heads, head_size)
                gate_block = lax.dynamic_slice_in_dim(fox_gates, key_start, block_rows, 0).T
                key_pos = key_start + jnp.arange(block_rows, dtype=jnp.int32)
                return softmax_update(
                    current,
                    query_heads,
                    own_gates,
                    query_pos,
                    key_block,
                    value_block,
                    gate_block,
                    key_pos,
                    score_scale,
                )

            def unchanged(current):
                return current

            return (lax.cond(key_start <= last_query, compute, unchanged, state_now), None)

        finished, _ = lax.scan(advance, running, jnp.arange(count // block_rows, dtype=jnp.int32))
        return finished

    top_final, total_final, weighted_final = attend(
        starting, sent_together((fox_key, fox_value), SP, 0, 1), jnp.int32(0)
    )
    fox_mix = (
        jnp.transpose(weighted_final / total_final[:, :, None], (1, 0, 2))
        .reshape(sequence_length, fox_heads * head_size)
        .astype(jnp.bfloat16)
    )
    ret_full, fox_full = rows_first((ret_out_weight, fox_out_weight), SP, (1, 1))
    mixed = summed_on_arrival(
        (
            jnp.dot(retention_mixed, ret_full, preferred_element_type=jnp.float32)
            + jnp.dot(fox_mix, fox_full, preferred_element_type=jnp.float32)
        ).astype(jnp.bfloat16),
        "tp",
        0,
    )
    return mixed.astype(jnp.bfloat16)


def solution(mesh):
    torus = Mesh(
        mesh.devices.reshape(mesh.shape["grp"], 32, 2, mesh.shape["tp"]),
        ("grp", "sp_0", "sp_1", "tp"),
    )
    return jax.shard_map(
        local,
        mesh=torus,
        in_specs=(
            P(GRP_SP, "tp"),
            P(),
            P(SP, "tp"),
            P(SP, "tp"),
            P(SP, "tp"),
            P(SP, "tp"),
            P(SP, "tp"),
            P(SP, "tp"),
            P("tp"),
            P(("grp", "tp"), None, None),
            P("tp"),
            P("grp", "tp"),
            P("tp", SP),
            P("tp", SP),
        ),
        out_specs=P(GRP_SP_TP, None),
        check_vma=False,
    )
```

profile of v0, /device:TPU:40, one launch (start us, length us, event | category | flops | bytes accessed | tf_op | source)
XLA Modules:
  0.0 495.9 jit_solution(9401134259431210037)
XLA Ops:
  6.6 1.5 concatenate.9
  8.1 1.1 copy.22
  9.2 1.0 broadcast_in_dim.40
  10.3 4.6 all-to-all-start
  14.8 0.6 pad_maximum_fusion.1
  15.4 0.2 all-gather.8.cloned.1.call-update
  15.7 14.3 %all-to-all-done = bf16[4,256,512]{1,2,0:T(8,128)(2,1)S(1)} async-done(((bf16[4,256,512]{1,2,0:T(8,128)(2,1)}), bf16[4,256,512]{1,2,0:T(8,128)(2,1)S(1)}, u32[]{:S(2)}, u32[]{:S(2)}) %all-to-all-start) | async-done | bytes 1048608 | tf_op jit(solution)/shard_map/all_to_all | solution.py:23
  30.0 0.3 multiply_reduce_fusion
  30.3 0.3 fusion.12
  30.7 138.3 %all-gather.6.cloned.1.call-done = bf16[2048,640]{1,0:T(8,128)(2,1)} async-done(((bf16[32,640]{1,0:T(8,128)(2,1)}), bf16[2048,640]{1,0:T(8,128)(2,1)}) %all-gather.6.cloned.1.call-update) | async-done | bytes 2621456 | tf_op jit(solution)/shard_map/all_gather | solution.py:35
  169.0 1.4 convolution_convert_fusion.1
  170.4 1.4 convolution_convert_fusion.2
  171.8 0.7 pad_maximum_fusion
  172.7 0.1 copy.26
  172.8 0.7 dynamic-slice_bitcast_fusion.1
  173.8 1.6 convolution_convert_fusion.4
  175.4 1.4 convolution_convert_fusion.3
  176.8 0.1 fusion.37
  176.9 55.8 %all-gather = bf16[64,32,64]{2,1,0:T(8,128)(2,1)S(1)} all-gather(bf16[2,32,64]{2,1,0:T(8,128)(2,1)S(1)} %fusion.37), channel_id=2, replica_groups=mesh['grp'=2,'sp_0'=32,'sp_1'=2,'tp'=4] {'sp_0'}, dimensions={0}, use_global_device_ids=true | all-gather | bytes 270336 | tf_op jit(solution)/shard_map/all_gather | solution.py:42
  232.8 2.6 all-gather.1
  235.4 0.7 fusion.13
  236.1 1.4 convolution_convert_fusion.5
  237.5 0.3 fusion.18
  237.8 0.4 fusion.49
  238.3 1.4 convolution_convert_fusion
  239.7 57.0 %all-gather.8.cloned.1.call-done = bf16[2048,256]{1,0:T(8,128)(2,1)} async-done(((bf16[32,256]{1,0:T(8,128)(2,1)}), bf16[2048,256]{1,0:T(8,128)(2,1)}) %all-gather.8.cloned.1.call-update) | async-done | bytes 1048592 | tf_op jit(solution)/shard_map/all_gather | solution.py:56
  296.8 1.5 fusion.23
  298.2 147.8 %all-gather.10.cloned.1.call-done = bf16[16384,256]{0,1:T(8,128)(2,1)} async-done(((bf16[256,256]{0,1:T(8,128)(2,1)}), bf16[16384,256]{0,1:T(8,128)(2,1)}) %all-gather.10.cloned.1.call-update) | async-done | bytes 8388624 | tf_op jit(solution)/shard_map/all_gather | solution.py:35
  446.1 5.8 %fusion.48 = (bf16[16384,128]{0,1:T(8,128)(2,1)}, bf16[16384,128]{0,1:T(8,128)(2,1)}) fusion(bf16[16384,256]{0,1:T(8,128)(2,1)} %all-gather.10.cloned.1.call-done), kind=kLoop, calls=%fused_computation.83 | loop fusion | bytes 16777216 | tf_op jit(solution)/shard_map/split | solution.py:36
  451.9 16.4 %while.15 = (s32[]{:T(128)}, f32[2,256]{1,0:T(2,128)S(1)}, f32[2,256]{1,0:T(2,128)S(1)}, f32[2,256,64]{1,2,0:T(8,128)S(1)}, s32[8]{0:T(128)S(1)}, /*index=5*/s32...) while((s32[]{:T(128)}, f32[2,256]{1,0:T(2,128)S(1)}, ...), condition=%wide.region_8.9_spmd.clone, body=%wide.region_3.8_spmd.clone.sunk | while | flops 278465792 | bytes 17209772 | solution.py:239
  451.9 0.6 dynamic_slice.23
  453.2 6.1 %conditional.3 = ((f32[2,256]{1,0:T(2,128)S(1)}, f32[2,256]{1,0:T(2,128)S(1)}, f32[2,256,64]{1,2,0:T(8,128)S(1)})) conditional(s32[]{:T(128)} %convert_element_type.113, (f32[2,256]{1,0:T(2,128)S(1)}, f32[2,256]{1,0:T(2,128)S(1)}, f32[2,256,64]{1,2,0:T(8,128)S(1)}) %tuple.39, (s32[]{:T(128)}, s32[]{:T(128)}, s32[]{:T(128)}, ...), branch_computations={%region_4.4_spmd, %region_5.7_spmd} | conditional | flops 278465792 | bytes 17208448 | solution.py:237
  453.9 0.8 dynamic-slice_bitcast_fusion
  454.7 0.5 broadcast_compare_fusion
  455.2 1.3 constant_dynamic-slice_fusion
  456.4 1.4 fusion.47
  457.9 0.6 fusion.3
  458.4 0.8 fusion.7
  459.3 0.6 dynamic_slice.23
  460.6 0.6 dynamic_slice.23
  461.9 0.6 dynamic_slice.23
  463.2 0.6 dynamic_slice.23
  464.4 0.6 dynamic_slice.23
  465.7 0.6 dynamic_slice.23
  467.0 0.6 dynamic_slice.23
  468.4 0.5 fusion.10
  468.8 19.6 %all_to_all.10 = bf16[4,64,2048]{2,1,0:T(8,128)(2,1)S(1)} all-to-all(bf16[4,64,2048]{2,1,0:T(8,128)(2,1)S(1)} %bitcast.68), channel_id=1, replica_groups=mesh['grp'=2,'sp_0'=32,'sp_1'=2,'tp'=4] {'tp'}, dimensions={0} | all-to-all | bytes 2097152 | tf_op jit(solution)/shard_map/all_to_all | solution.py:71
  488.4 0.9 reduce_sum.51
  (59 shorter events, 1.0 us)
Async XLA Ops:
  6.5 8.3 %copy-start.3 = (bf16[128,32]{0,1:T(8,128)(2,1)S(1)}, bf16[128,32]{0,1:T(8,128)(2,1)}, u32[]{:S(2)}) copy-start(bf16[128,32]{0,1:T(8,128)(2,1)} %param.31) | copy-start | bytes 24580
  6.5 8.3 %copy-start.4 = (bf16[128,32]{0,1:T(8,128)(2,1)S(1)}, bf16[128,32]{0,1:T(8,128)(2,1)}, u32[]{:S(2)}) copy-start(bf16[128,32]{0,1:T(8,128)(2,1)} %param.30) | copy-start | bytes 24580
  6.6 23.8 %copy-start.2 = (f32[2048]{0:T(1024)S(1)}, f32[2048]{0:T(1024)}, u32[]{:S(2)}) copy-start(f32[2048]{0:T(1024)} %param.19) | copy-start | bytes 24580
  6.6 162.4 %all-gather.6.cloned.1.call-start = ((), (), s32[]{:S(2)}) async-start(), calls=%async_computation.2 | async-start | bytes 2662400 | tf_op jit(solution)/shard_map/all_gather | solution.py:35
  10.3 19.7 %all-to-all-start = ((bf16[4,256,512]{1,2,0:T(8,128)(2,1)}), bf16[4,256,512]{1,2,0:T(8,128)(2,1)S(1)}, u32[]{:S(2)}, u32[]{:S(2)}) async-start(bf16[4,256,512]{1,2,0:T(8,128)(2,1)} %broadcast_in_dim.40), calls=%async_computation | async-start | bytes 2097152 | tf_op jit(solution)/shard_map/all_to_all | solution.py:23
  14.8 281.9 %all-gather.8.cloned.1.call-start = ((), (), s32[]{:S(2)}) async-start(), calls=%async_computation.3 | async-start | bytes 1064960 | tf_op jit(solution)/shard_map/all_gather | solution.py:56
  15.6 430.5 %all-gather.10.cloned.1.call-start = ((), (), s32[]{:S(2)}) async-start(), calls=%async_computation.4 | async-start | bytes 8519680 | tf_op jit(solution)/shard_map/all_gather | solution.py:35
  30.3 142.2 %copy-start.6 = (f32[128]{0:T(128)S(1)}, f32[128]{0:T(128)}, u32[]{:S(2)}) copy-start(f32[128]{0:T(128)} %param.28) | copy-start | bytes 1540
  30.3 142.3 %copy-start.5 = (f32[2]{0:T(128)S(1)}, f32[2]{0:T(128)}, u32[]{:S(2)}) copy-start(f32[2]{0:T(128)} %param.26) | copy-start | bytes 28
  235.3 2.1 copy-start.1
  451.9 16.4 %copy-start = (bf16[2048,256]{1,0:T(8,128)(2,1)S(1)}, bf16[2048,256]{1,0:T(8,128)(2,1)}, u32[]{:S(2)}) copy-start(bf16[2048,256]{1,0:T(8,128)(2,1)} %all-gather.8.cloned.1.call-done) | copy-start | bytes 3145732
Sparse Core Ops, SparseCore 0:
  9.5 159.4 all-gather.5
  171.1 125.5 all-gather.7
  298.8 147.2 all-gather.9
where the time goes:
time: 501 us; the launch traced here: 496 us
  waiting for transfers between devices  358 us (71%)
  blocking collectives  78 us (16%)
  local copies, waits for them, and re-layouts  17.2 us (3%)
  matrix products  14.3 us (3%)
  between operations  13.3 us (3%)
  loops' own time  6.36 us (1%)
    all_gather x2, waiting for transfers between devices, sent_together(): result = lax.all_gather(both, axis, axis=dim, tiled=True)  286 us
    all_gather x2, blocking collectives, all_blocks(): blocks = lax.all_gather(blocks, axes[k])  58.4 us
    all_gather x1, waiting for transfers between devices, rows_first(): lax.all_gather(both, axis, axis=0, tiled=True)  57 us
    all_to_all x1, blocking collectives, summed_on_arrival(): lax.all_to_all(blocks, axis, split_axis=0, concat_axis=0, tiled=True)  19.6 us
    all_to_all x1, waiting for transfers between devices, from_everyone(): lax.all_to_all(jnp.broadcast_to(array[None], (count, *array.shape)), axis...  14.3 us
  transfers between devices with their start and end apart: 4, of which 4 were waited for; matrix products, arithmetic and copies ran while one was open for 3% of the time, Pallas kernels for 0%

commit v1 on v0

v1 whole, which is shorter than its diff:
```python
import jax
import jax.numpy as jnp
from jax import lax
from jax.experimental import pallas as pl
from jax.experimental.pallas import tpu as pltpu
from jax.sharding import Mesh
from jax.sharding import PartitionSpec as P

SP = ("sp_0", "sp_1")
GRP_SP = ("grp", "sp_0", "sp_1")
GRP_SP_TP = ("grp", "sp_0", "sp_1", "tp")

EPSILON = 1e-06
LOG2E = 1.4426950408889634

SMALL_WEIGHT = 2.0**18
QUERY_WEIGHT = 2.0**12
FOX_OUT_WEIGHT = 2.0**15
KEY_VALUE = 2.0**7
STATE = 2.0**-9
STATE_LOW = 2.0**11


def head_norm(raw, gain):
    center = raw - jnp.mean(raw, axis=-1, keepdims=True)
    spread = jnp.mean(center * center, axis=-1, keepdims=True)
    return (center * lax.rsqrt(spread + EPSILON) * gain).astype(jnp.bfloat16)


def attention_kernel(place, query, gathered, gates, out, *, scale, value_scale):
    chunk = query.shape[0]
    width = query.shape[1]
    q = query[...]

    def logits_of(j):
        pairs = gathered[j]
        s = lax.dot_general(q, pairs, (((1,), (1,)), ((), ())), preferred_element_type=jnp.float32)
        return s * scale - gates[j], pairs

    own = place[0]
    t, pairs = logits_of(own)
    row = lax.broadcasted_iota(jnp.int32, (chunk, chunk), 0)
    col = lax.broadcasted_iota(jnp.int32, (chunk, chunk), 1)
    t = jnp.where(col <= row, t, -jnp.inf)
    top = jnp.max(t, axis=1, keepdims=True)
    p = jnp.exp2(t - top)
    total = jnp.sum(p, axis=1, keepdims=True)
    mixed = jnp.dot(p.astype(jnp.bfloat16), pairs, preferred_element_type=jnp.float32)

    def step(j, state):
        top, total, mixed = state
        t, pairs = logits_of(j)
        new = jnp.maximum(top, jnp.max(t, axis=1, keepdims=True))
        p = jnp.exp2(t - new)
        keep = jnp.exp2(top - new)
        total = total * keep + jnp.sum(p, axis=1, keepdims=True)
        mixed = mixed * keep + jnp.dot(
            p.astype(jnp.bfloat16), pairs, preferred_element_type=jnp.float32
        )
        return new, total, mixed

    _, total, mixed = lax.fori_loop(0, own, step, (top, total, mixed))
    out[...] = ((mixed * value_scale) / total)[:, width // 2 :].astype(out.dtype)


def attend(place, query, gathered, gates, scale):
    chunk, head = query.shape
    padded = jnp.concatenate([query, jnp.zeros_like(query)], axis=1)
    vmem = pl.BlockSpec(memory_space=pltpu.VMEM)
    return pl.pallas_call(
        lambda *refs: attention_kernel(
            *refs, scale=scale * LOG2E / KEY_VALUE, value_scale=1.0 / KEY_VALUE
        ),
        out_shape=jax.ShapeDtypeStruct((chunk, head), jnp.bfloat16),
        in_specs=[pl.BlockSpec(memory_space=pltpu.SMEM), vmem, vmem, vmem],
        out_specs=vmem,
        compiler_params=pltpu.CompilerParams(vmem_limit_bytes=40 * 2**20),
        name="attend",
    )(place[None], padded, gathered, gates)


def local(
    tokens,
    norm_gain,
    ret_query_weight,
    ret_key_weight,
    ret_value_weight,
    fox_query_weight,
    fox_key_weight,
    fox_value_weight,
    ret_decay,
    ret_state,
    head_norm_gain,
    fox_gates,
    ret_out_weight,
    fox_out_weight,
):
    f32, bf16, f16 = jnp.float32, jnp.bfloat16, jnp.float16
    chip, core = lax.axis_index("sp_0"), lax.axis_index("sp_1")
    chips, cores, tp = (lax.axis_size(a) for a in ("sp_0", "sp_1", "tp"))
    rows = tokens.shape[0]
    chunk = rows * cores
    swap = [(k, cores - 1 - k) for k in range(cores)]

    sent = jnp.broadcast_to(tokens[None], (cores * tp, *tokens.shape))
    arrived = lax.all_to_all(sent, ("sp_1", "tp"), 0, 0, tiled=True)
    wide = arrived.reshape(cores, tp, rows, -1).transpose(0, 2, 1, 3).reshape(chunk, -1)

    def by_head(weight, scale):
        split = weight.astype(f32).reshape(weight.shape[0], cores, -1) * scale
        return jnp.moveaxis(split, 1, 0)

    def out_by_head(weight, scale):
        split = weight.astype(f32).reshape(cores, -1, weight.shape[1]) * scale
        return jnp.swapaxes(split, 1, 2)

    sections = (
        (out_by_head, ret_out_weight, SMALL_WEIGHT),
        (out_by_head, fox_out_weight, FOX_OUT_WEIGHT),
        (by_head, fox_key_weight, SMALL_WEIGHT),
        (by_head, fox_value_weight, SMALL_WEIGHT),
        (by_head, fox_query_weight, QUERY_WEIGHT),
        (by_head, ret_value_weight, SMALL_WEIGHT),
        (by_head, ret_key_weight, SMALL_WEIGHT),
        (by_head, ret_query_weight, SMALL_WEIGHT),
    )
    pieces = [make(weight, scale) for make, weight, scale in sections]
    packed = jnp.concatenate(pieces, axis=2).astype(f16)
    packed = jnp.pad(packed, ((0, 0), (0, 0), (0, -packed.shape[2] % 128)))
    packed = lax.all_to_all(packed, "sp_1", 0, 0, tiled=True).reshape(-1, packed.shape[2])
    weights = lax.all_gather(packed, "sp_0", axis=0, tiled=True)
    back = jnp.concatenate(
        [jnp.full((p.shape[2],), 1.0 / s, f32) for p, (_, _, s) in zip(pieces, sections)]
    )
    weights = (weights[:, : back.shape[0]].astype(f32) * back).astype(bf16)
    out_width = pieces[0].shape[2] + pieces[1].shape[2]
    out_own = weights[:, :out_width]
    out_other = lax.ppermute(out_own, "sp_1", swap)

    widened = wide.astype(f32)
    normed = (
        widened
        * lax.rsqrt(jnp.mean(widened * widened, axis=-1, keepdims=True) + EPSILON)
        * norm_gain
    ).astype(bf16)
    projected = jnp.dot(normed, weights[:, out_width:], preferred_element_type=f32).astype(bf16)
    ends, at = [], 0
    for piece in pieces[2:]:
        at += piece.shape[2]
        ends.append(at)
    pair_width = ends[1]
    pairs = projected[:, :pair_width]
    _, _, fox_query, ret_value, ret_key, ret_query = jnp.split(projected, ends[:-1], axis=1)

    decay = lax.dynamic_index_in_dim(ret_decay, core, 0, False)
    key_scale = ret_key.shape[1] ** (-0.5)
    at = jnp.arange(chunk, dtype=f32)
    trailing = jnp.exp((chunk - 1.0 - at) * decay) * key_scale
    summary = lax.dot_general(
        ret_key.astype(f32) * trailing[:, None],
        ret_value.astype(f32),
        (((0,), (0,)), ((), ())),
        preferred_element_type=f32,
    )
    scaled = summary * STATE
    high = lax.reduce_precision(scaled, 5, 10)
    low = (scaled - high) * STATE_LOW
    payload = jnp.concatenate(
        [pairs.astype(f32) * KEY_VALUE, jnp.concatenate([high, low], axis=1)], axis=0
    ).astype(f16)
    gathered = lax.all_gather(payload, "sp_0", axis=0, tiled=False)

    gates = lax.dynamic_index_in_dim(fox_gates, core, 1, False)
    reference_gate = lax.dynamic_index_in_dim(gates, chip * chunk, 0, True)
    gates = ((gates - reference_gate) * LOG2E).reshape(chips, 1, chunk)
    fox_mix = attend(
        chip.astype(jnp.int32),
        fox_query,
        gathered[:, :chunk, :].astype(f32).astype(bf16),
        gates,
        fox_query.shape[1] ** (-0.5)
    )

    value_size = ret_value.shape[1]
    summaries = gathered[:, chunk:, :].astype(f32)
    summaries = summaries[:, :, :value_size] + summaries[:, :, value_size:] * (1.0 / STATE_LOW)
    ids = jnp.arange(chips, dtype=jnp.int32)
    distance = jnp.maximum(chip - ids - 1, 0).astype(f32) * chunk
    share = jnp.where(ids < chip, jnp.exp(distance * decay), 0.0) * (1.0 / STATE)
    before = jnp.sum(summaries * share[:, None, None], axis=0)
    first = (chip * chunk).astype(f32)
    state = lax.dynamic_index_in_dim(ret_state, core, 0, False)
    entering = jnp.exp(first * decay) * state + before
    spread = at[:, None] - at[None, :]
    within = jnp.where(spread >= 0, jnp.exp(jnp.maximum(spread, 0.0) * decay), 0.0) * key_scale
    near = (
        lax.dot_general(
            ret_query, ret_key, (((1,), (1,)), ((), ())), preferred_element_type=f32
        )
        * within
    )
    inner = jnp.dot(near, ret_value.astype(f32), preferred_element_type=f32)
    carried = jnp.dot(
        ret_query.astype(f32), entering, preferred_element_type=f32, precision=lax.Precision.HIGHEST
    )
    carried = carried * jnp.exp((at + 1.0) * decay)[:, None]
    gain = lax.dynamic_slice_in_dim(head_norm_gain, core * value_size, value_size)
    ret_mix = head_norm(inner + carried, gain)

    mix = jnp.concatenate([ret_mix, fox_mix], axis=1)
    mine = lax.dynamic_slice_in_dim(mix, core * rows, rows, 0)
    theirs = lax.dynamic_slice_in_dim(mix, (cores - 1 - core) * rows, rows, 0)
    other = lax.ppermute(theirs, "sp_1", swap)

    def project(rows_in, weight):
        return lax.dot_general(
            rows_in, weight, (((1,), (1,)), ((), ())), preferred_element_type=f32
        )

    partial = (project(mine, out_own) + project(other, out_other)).astype(bf16)
    blocks = partial.reshape(tp, rows // tp, -1)
    arrived = lax.all_to_all(blocks, "tp", 0, 0, tiled=True)
    return arrived.astype(f32).sum(axis=0).astype(bf16)


def solution(mesh):
    torus = Mesh(
        mesh.devices.reshape(mesh.shape["grp"], mesh.shape["sp"] // 2, 2, mesh.shape["tp"]),
        ("grp", "sp_0", "sp_1", "tp"),
    )
    return jax.shard_map(
        local,
        mesh=torus,
        in_specs=(
            P(GRP_SP, "tp"),
            P(),
            P(SP, "tp"),
            P(SP, "tp"),
            P(SP, "tp"),
            P(SP, "tp"),
            P(SP, "tp"),
            P(SP, "tp"),
            P("tp"),
            P(("grp", "tp"), None, None),
            P("tp"),
            P("grp", "tp"),
            P("tp", SP),
            P("tp", SP),
        ),
        out_specs=P(GRP_SP_TP, None),
        check_vma=False,
    )
```

time: 501 us -> 263 us (0.52)
  waiting for transfers between devices: 358 us -> 0.72 us
  blocking collectives: 78 us -> 215 us
  between operations: 13.3 us -> 1.66 us
  other arithmetic: 4.36 us -> 14.1 us
  matrix products: 14.3 us -> 6.09 us
  loops' own time: 6.36 us -> 0 us
    all_gather x3 -> x0, waiting for transfers between devices: 343 us -> none  [the longest x2 286 us: sent_together(): result = lax.all_gather(both, axis, axis=dim, tiled=True)]
    all_gather x2, blocking collectives: 58.4 us -> 192 us  [the longest x1 108 us: local(): weights = lax.all_gather(packed, 'sp_0', axis=0, tiled=True)]
    all_to_all x1, waiting for transfers between devices: 14.3 us -> 0.01 us  [local(): arrived = lax.all_to_all(sent, ('sp_1', 'tp'), 0, 0, tiled=True)]
    dot_general x14 -> x6, matrix products: 14.3 us -> 6.09 us  [the longest x1 2.52 us: local(): inner = jnp.dot(near, ret_value.astype(f32), preferred_element_type=f32)]
    another operation x9 -> x0, loops' own time: 6.36 us -> none  [the longest x1 5.53 us: attend(): lax.scan(advance, running, jnp.arange(count // block_rows, dtype=jnp.int32))]
    another operation x0 -> x8, other arithmetic: none -> 5.62 us
    split x1, local copies, waits for them, and re-layouts: 5.81 us -> 0.72 us  [local(): jnp.split(projected, ends[:-1], axis=1)]
    all_to_all x1 -> x2, blocking collectives: 19.6 us -> 23.2 us  [the longest x1 19.4 us: local(): arrived = lax.all_to_all(blocks, 'tp', 0, 0, tiled=True)]
  transfers between devices with their start and end apart: 4 -> 3, of which waited for: 4 -> 1; matrix products, arithmetic and copies ran while one was open for 3% -> 8% of each run, Pallas kernels for 0% -> 0%
where the time goes in v1:
time: 263 us; the launch traced here: 262 us
  blocking collectives  215 us (82%)
  local copies, waits for them, and re-layouts  14.8 us (6%)
  other arithmetic  14.1 us (5%)
  starting transfers between devices  8.49 us (3%)
  matrix products  6.09 us (2%)
    all_gather x1, blocking collectives, local(): weights = lax.all_gather(packed, 'sp_0', axis=0, tiled=True)  108 us
    all_gather x1, blocking collectives, local(): gathered = lax.all_gather(payload, 'sp_0', axis=0, tiled=False)  83.5 us
    all_to_all x1, blocking collectives, local(): arrived = lax.all_to_all(blocks, 'tp', 0, 0, tiled=True)  19.4 us
    another operation x8, other arithmetic  5.62 us
    unnamed x23, local copies, waits for them, and re-layouts  5.58 us
  transfers between devices with their start and end apart: 3, of which 1 were waited for; matrix products, arithmetic and copies ran while one was open for 8% of the time, Pallas kernels for 0%

profile of v1, /device:TPU:40, one launch (start us, length us, event | category | flops | bytes accessed | tf_op | source)
XLA Modules:
  0.0 261.8 jit_solution(4927740790396315758)
XLA Ops:
  0.0 0.7 multiply_convert_fusion.7
  0.7 0.1 mul.281
  0.8 0.7 multiply_convert_fusion.8
  1.5 0.1 mul.279
  1.6 0.7 multiply_convert_fusion.9
  2.3 0.1 mul.277
  2.4 0.7 multiply_convert_fusion.10
  3.1 0.7 multiply_convert_fusion.12
  3.9 0.7 multiply_convert_fusion.11
  4.7 0.7 multiply_convert_fusion.14
  5.5 0.7 multiply_convert_fusion.13
  6.3 0.3 concatenate.29
  6.7 3.8 %all_to_all.15 = f16[2,32,512]{2,1,0:T(8,128)(2,1)S(1)} all-to-all(f16[2,32,512]{2,1,0:T(8,128)(2,1)S(1)} %pad.5.clone), channel_id=1, replica_groups=mesh['grp'=2,'sp_0'=32,'sp_1'=2,'tp'=4] {'sp_1'}, dimensions={0} | all-to-all | bytes 131072 | tf_op jit(solution)/shard_map/all_to_all | solution.py:130
  10.5 2.4 broadcast_in_dim.8
  12.9 4.6 %all-to-all-start = ((bf16[8,256,512]{2,1,0:T(8,128)(2,1)}), bf16[8,256,512]{2,1,0:T(8,128)(2,1)S(1)}, u32[]{:S(2)}, u32[]{:S(2)}) async-start(bf16[8,256,512]{2,1,0:T(8,128)(2,1)} %broadcast_in_dim.8), calls=%async_computation | async-start | bytes 4194304 | tf_op jit(solution)/shard_map/all_to_all | solution.py:106
  17.5 108.3 %all-gather.2 = f16[2048,512]{1,0:T(8,128)(2,1)S(1)} all-gather(f16[64,512]{1,0:T(8,128)(2,1)S(1)} %bitcast.41), channel_id=1, replica_groups=mesh['grp'=2,'sp_0'=32,'sp_1'=2,'tp'=4] {'sp_0'}, dimensions={0}, use_global_device_ids=true | all-gather | bytes 2162688 | tf_op jit(solution)/shard_map/all_gather | solution.py:131
  125.9 0.4 multiply_convert_fusion
  126.3 1.3 copy-done.1
  127.7 2.0 collective-permute-start.1
  129.7 0.7 dynamic_slice.25
  130.4 0.6 multiply_exponential_fusion
  131.0 0.6 exponential_multiply_fusion
  133.1 0.6 dynamic_slice.29
  133.7 0.7 subtract_multiply_fusion
  134.4 0.5 multiply_reduce_fusion
  135.0 0.6 convert_element_type.128
  135.5 2.7 %copy.36 = f32[2,256,4,512]{3,2,1,0:T(4,128)S(1)} copy(f32[2,256,4,512]{3,1,2,0:T(8,128)S(1)} %bitcast.37) | data formatting | bytes 8388608 | tf_op jit(solution)/shard_map/convert_element_type | solution.py:140
  138.3 2.0 copy.46
  140.3 1.3 fusion.6
  141.6 0.7 split.19
  142.3 0.3 reduce-precision_convert_fusion
  142.8 83.5 %all-gather.3 = f16[32,544,128]{2,1,0:T(8,128)(2,1)S(1)} all-gather(f16[1,544,128]{2,1,0:T(8,128)(2,1)S(1)} %pad_maximum_fusion), channel_id=1, replica_groups=mesh['grp'=2,'sp_0'=32,'sp_1'=2,'tp'=4] {'sp_0'}, dimensions={0}, use_global_device_ids=true | all-gather | bytes 4595712 | tf_op jit(solution)/shard_map/all_gather | solution.py:171
  226.4 3.0 %convert_convert_fusion.refs_2_ = bf16[32,512,128]{2,1,0:T(8,128)(2,1)} fusion(f16[32,544,128]{2,1,0:T(8,128)(2,1)S(1)} %all-gather.3), kind=kLoop, calls=%fused_computation | loop fusion | flops 4194304 | bytes 8388608 | tf_op jit(solution)/shard_map/convert_element_type | solution.py:179
  229.4 0.2 fusion.19
  229.7 1.0 convolution_multiply_fusion.1
  230.7 2.5 fusion.51
  233.2 0.2 multiply_reduce_fusion.1
  233.5 0.9 concatenate.34.refs_1_
  234.4 2.2 copy-done
  236.6 0.9 attend.1
  237.5 0.2 multiply_convert_fusion.5
  237.7 0.1 fusion.35
  237.9 2.0 collective-permute-start
  239.8 0.5 fusion.37
  240.3 0.7 collective-permute-done
  241.0 0.4 fusion
  241.5 19.4 %all_to_all.16 = bf16[4,64,2048]{2,1,0:T(8,128)(2,1)S(1)} all-to-all(bf16[4,64,2048]{2,1,0:T(8,128)(2,1)S(1)} %bitcast.39), channel_id=1, replica_groups=mesh['grp'=2,'sp_0'=32,'sp_1'=2,'tp'=4] {'tp'}, dimensions={0} | all-to-all | bytes 2097152 | tf_op jit(solution)/shard_map/all_to_all | solution.py:222
  260.9 0.9 reduce_sum.61
  (40 shorter events, 0.9 us)
Async XLA Ops:
  10.5 115.4 %copy-start.6 = (f32[448]{0:T(512)S(1)}, f32[448]{0:T(512)}, u32[]{:S(2)}) copy-start(f32[448]{0:T(512)} %constant.39.clone.1) | copy-start | bytes 5380
  12.9 121.5 %all-to-all-start = ((bf16[8,256,512]{2,1,0:T(8,128)(2,1)}), bf16[8,256,512]{2,1,0:T(8,128)(2,1)S(1)}, u32[]{:S(2)}, u32[]{:S(2)}) async-start(bf16[8,256,512]{2,1,0:T(8,128)(2,1)} %broadcast_in_dim.8), calls=%async_computation | async-start | bytes 4194304 | tf_op jit(solution)/shard_map/all_to_all | solution.py:106
  17.5 112.2 %copy-start.8 = (f32[2]{0:T(128)S(1)}, f32[2]{0:T(128)}, u32[]{:S(2)}) copy-start(f32[2]{0:T(128)} %param.22) | copy-start | bytes 28
  17.5 115.5 %copy-start.9 = (f32[128]{0:T(128)S(1)}, f32[128]{0:T(128)}, u32[]{:S(2)}) copy-start(f32[128]{0:T(128)} %param.24) | copy-start | bytes 1540
  17.5 115.6 %copy-start.4 = (f32[16384,2]{0,1:T(2,128)S(1)}, f32[16384,2]{0,1:T(2,128)}, u32[]{:S(2)}) copy-start(f32[16384,2]{0,1:T(2,128)} %param.25) | copy-start | bytes 393220
  126.3 1.4 copy-start.1
  127.7 112.6 %collective-permute-start.1 = (bf16[2048,128]{1,0:T(8,128)(2,1)S(1)}, bf16[2048,128]{1,0:T(8,128)(2,1)S(1)}, u32[]{:S(2)}, u32[]{:S(2)}) collective-permute-start(bf16[2048,128]{1,0:T(8,128)(2,1)S(1)} %slice.39), channel_id=1, source_target_pairs={{0,4},{4,0},{1,5},{5,1},{2,6},{6,2},{3,7},{7,3},{8,12},{12,8},{9,1... | collective-permute-start | bytes 1572872 | tf_op jit(solution)/shard_map/ppermute | solution.py:138
  138.2 2.0 copy-start.2
  138.2 2.0 copy-start.7
  141.6 88.1 %copy-start.3 = (bf16[512,320]{1,0:T(8,128)(2,1)}, bf16[512,320]{1,0:T(8,128)(2,1)S(1)}, u32[]{:S(2)}) copy-start(bf16[512,320]{1,0:T(8,128)(2,1)S(1)} %fusion.6) | copy-start | bytes 983044
  226.4 3.3 %copy-start.5 = (f32[2,32,64]{2,1,0:T(8,128)S(1)}, f32[2,32,64]{2,1,0:T(8,128)}, u32[]{:S(2)}) copy-start(f32[2,32,64]{2,1,0:T(8,128)} %param.23) | copy-start | bytes 49156
  234.4 2.2 copy-start
  237.9 3.2 %collective-permute-start = (bf16[256,128]{1,0:T(8,128)(2,1)S(1)}, bf16[256,128]{1,0:T(8,128)(2,1)S(1)}, u32[]{:S(2)}, u32[]{:S(2)}) collective-permute-start(bf16[256,128]{1,0:T(8,128)(2,1)S(1)} %fusion.35), channel_id=1, source_target_pairs={{0,4},{4,0},{1,5},{5,1},{2,6},{6,2},{3,7},{7,3},{8,12},{12,8},{9,1... | collective-permute-start | bytes 196616 | tf_op jit(solution)/shard_map/ppermute | solution.py:213

commit v2 on v1

v2 whole, which is shorter than its diff:
```python
import jax
import jax.numpy as jnp
from jax import lax
from jax.experimental import pallas as pl
from jax.experimental.pallas import tpu as pltpu
from jax.sharding import Mesh
from jax.sharding import PartitionSpec as P


SP = ("sp_0", "sp_1")
CHIP = ("sp_1", "tp")
GRP_SP = ("grp", "sp_0", "sp_1")
GRP_SP_TP = ("grp", "sp_0", "sp_1", "tp")

EPSILON = 1e-06
LOG2E = 1.4426950408889634
MIB = 2**20

SMALL_WEIGHT = 2.0**18
QUERY_WEIGHT = 2.0**12
FOX_OUT_WEIGHT = 2.0**15
KEY_VALUE = 2.0**7
STATE = 2.0**-9
STATE_LOW = 2.0**8

VMEM = pl.BlockSpec(memory_space=pltpu.VMEM)
SMEM = pl.BlockSpec(memory_space=pltpu.SMEM)
NT = (((1,), (1,)), ((), ()))
TN = (((0,), (0,)), ((), ()))


def dot(a, b, dims=(((1,), (0,)), ((), ()))):
    return lax.dot_general(a, b, dims, preferred_element_type=jnp.float32)


def two_terms(x):
    high = x.astype(jnp.bfloat16)
    return high, (x - high.astype(jnp.float32)).astype(jnp.bfloat16)


def column_of(count):
    return lax.broadcasted_iota(jnp.int32, (count, 1), 0).astype(jnp.float32)


def pack_kernel(out_ret, out_fox, fk, fv, fq, rv, rk, rq, packed):
    f32 = jnp.float32
    heads = packed.shape[0]

    def columns(ref, h):
        size = ref.shape[1] // heads
        return ref[...].astype(f32)[:, h * size : (h + 1) * size]

    for h in range(heads):
        parts = [columns(ref, h) for ref in (out_ret, out_fox, fk, fv, fq, rv, rk, rq)]
        joined = jnp.concatenate(parts, axis=1)
        blank = packed.shape[2] - joined.shape[1]
        joined = jnp.concatenate([joined, jnp.zeros((joined.shape[0], blank), f32)], axis=1)
        packed[h] = joined.astype(packed.dtype)


def project_kernel(place, decays, tokens, gains, weights, query, values, keys, queries, payload, *, key, cores):
    f32, bf16 = jnp.float32, jnp.bfloat16
    rows, width = tokens.shape[1:]
    parts, value = tokens.shape[0] // cores, 2 * key
    for c in range(cores):
        square = jnp.zeros((rows, 1), f32)
        for k in range(parts):
            x = tokens[c * parts + k].astype(f32)
            square = square + jnp.sum(x * x, axis=1, keepdims=True)
        factor = lax.rsqrt(square * (1.0 / (parts * width)) + EPSILON)
        total = jnp.zeros((rows, weights.shape[1]), f32)
        for k in range(parts):
            x = tokens[c * parts + k].astype(f32)
            normed = (x * factor * gains[k]).astype(bf16)
            total = total + dot(normed, weights[k * width : (k + 1) * width, :])
        total = total.astype(bf16)
        at = slice(c * rows, (c + 1) * rows)
        payload[at, :] = total[:, : 2 * value].astype(f32) * KEY_VALUE
        lane = lax.broadcasted_iota(jnp.int32, (rows, 2 * value), 1)
        mixed = total[:, 2 * value : 4 * value].astype(f32)
        query[at, :] = jnp.where(lane < value, mixed, 0.0).astype(bf16)
        values[at, :] = total[:, 3 * value : 4 * value]
        keys[at, :] = total[:, 4 * value : 4 * value + key]
        queries[at, :] = total[:, 4 * value + key : 4 * value + 2 * key]
    chunk = rows * cores
    trailing = jnp.exp((chunk - 1.0 - column_of(chunk)) * decays[place[1]]) * key ** (-0.5)
    high, low = two_terms(keys[...].astype(f32) * trailing)
    summary = (dot(high, values[...], TN) + dot(low, values[...], TN)) * STATE
    high = summary.astype(bf16).astype(f32)
    payload[chunk:, :] = jnp.concatenate([high, (summary - high) * STATE_LOW], axis=1)


def mix_kernel(place, decays, query, values, keys, queries, gathered, gates, state, gains, mix, *, key):
    f32, bf16 = jnp.float32, jnp.bfloat16
    chunk, value = query.shape[0], 2 * key
    own, head = place[0], place[1]
    decay = decays[head]
    attending = query[...]
    scale = value ** (-0.5) * LOG2E / KEY_VALUE
    base = jnp.max(gates[head, own], axis=1, keepdims=True)

    def logits_of(j):
        pairs = gathered[j, :chunk, :]
        return dot(attending, pairs, NT) * scale - (gates[head, j] - base) * LOG2E, pairs

    row = lax.broadcasted_iota(jnp.int32, (chunk, chunk), 0)
    col = lax.broadcasted_iota(jnp.int32, (chunk, chunk), 1)
    t, pairs = logits_of(own)
    t = jnp.where(col <= row, t, -jnp.inf)
    top = jnp.max(t, axis=1, keepdims=True)
    p = jnp.exp2(t - top)
    total = jnp.sum(p, axis=1, keepdims=True)
    mixed = dot(p.astype(bf16), pairs)

    ones = jnp.ones((1, 2 * value), f32)
    per_chunk = jnp.exp(ones * (chunk * decay))

    def step(j, carry):
        top, total, mixed, memory = carry
        t, pairs = logits_of(j)
        new = jnp.maximum(top, jnp.max(t, axis=1, keepdims=True))
        p = jnp.exp2(t - new)
        keep = jnp.exp2(top - new)
        total = total * keep + jnp.sum(p, axis=1, keepdims=True)
        mixed = mixed * keep + dot(p.astype(bf16), pairs)
        memory = memory * per_chunk + gathered[j, chunk:, :].astype(f32)
        return new, total, mixed, memory

    memory = jnp.zeros((key, 2 * value), f32)
    _, total, mixed, memory = lax.fori_loop(0, own, step, (top, total, mixed, memory))
    fox = (mixed * (1.0 / KEY_VALUE) / total)[:, value:]

    memory = (memory[:, :value] + memory[:, value:] * (1.0 / STATE_LOW)) * (1.0 / STATE)
    first = (own * chunk).astype(f32)
    entering = jnp.exp(ones[:, :value] * (first * decay)) * state[head] + memory
    ret_query = queries[...]
    spread = (row - col).astype(f32)
    within = jnp.where(col <= row, jnp.exp(jnp.maximum(spread, 0.0) * decay), 0.0)
    near = dot(ret_query, keys[...], NT) * within * key ** (-0.5)
    high, low = two_terms(entering)
    carried = dot(ret_query, high) + dot(ret_query, low)
    raw = dot(near.astype(bf16), values[...]) + carried * jnp.exp((column_of(chunk) + 1.0) * decay)
    center = raw - jnp.mean(raw, axis=1, keepdims=True)
    variance = jnp.mean(center * center, axis=1, keepdims=True)
    ret = center * lax.rsqrt(variance + EPSILON) * gains[head]
    mix[...] = jnp.concatenate([ret, fox], axis=1).astype(bf16)


def output_kernel(mixes, weights, out, *, cores):
    parts = mixes.shape[0] // cores
    summed = jnp.zeros(out.shape, jnp.float32)
    for k in range(parts):
        partial = sum(
            dot(mixes[c * parts + k], weights[c * parts + k], NT) for c in range(cores)
        )
        summed = summed + partial.astype(jnp.bfloat16).astype(jnp.float32)
    out[...] = summed.astype(out.dtype)


def kernel(body, out_shape, in_specs, limit):
    many = isinstance(out_shape, tuple)
    return pl.pallas_call(
        body,
        out_shape=out_shape,
        in_specs=in_specs,
        out_specs=(VMEM,) * len(out_shape) if many else VMEM,
        compiler_params=pltpu.CompilerParams(vmem_limit_bytes=limit * MIB),
    )


def layer(
    tokens,
    norm_gain,
    ret_query_weight,
    ret_key_weight,
    ret_value_weight,
    fox_query_weight,
    fox_key_weight,
    fox_value_weight,
    ret_decay,
    ret_state,
    head_norm_gain,
    fox_gates,
    ret_out_weight,
    fox_out_weight,
):
    f32, bf16, f16 = jnp.float32, jnp.bfloat16, jnp.float16
    chip, core = lax.axis_index("sp_0"), lax.axis_index("sp_1")
    chips, cores, tp = (lax.axis_size(a) for a in ("sp_0", "sp_1", "tp"))
    rows, width = tokens.shape
    chunk = rows * cores
    key, value = ret_query_weight.shape[1] // cores, ret_value_weight.shape[1] // cores
    place = jnp.stack([chip, core]).astype(jnp.int32)

    sent = jnp.broadcast_to(tokens[None], (cores * tp, rows, width))
    wide = lax.all_to_all(sent, CHIP, 0, 0, tiled=True)

    shard = fox_key_weight.shape[0]
    lanes = 2 * value + 4 * value + 2 * key
    padded = lanes + -lanes % 128
    packed = pl.pallas_call(
        pack_kernel,
        out_shape=jax.ShapeDtypeStruct((cores, shard, padded), bf16),
        grid=(1,),
        in_specs=[
            pl.BlockSpec((shard, size * cores), lambda i: (0, 0))
            for size in (value,) * 6 + (key,) * 2
        ],
        out_specs=pl.BlockSpec((cores, shard, padded), lambda i: (0, 0, 0)),
        name="pack",
    )(
        ret_out_weight.T,
        fox_out_weight.T,
        fox_key_weight,
        fox_value_weight,
        fox_query_weight,
        ret_value_weight,
        ret_key_weight,
        ret_query_weight,
    )
    packed = lax.all_to_all(packed, "sp_1", 0, 0, tiled=True).reshape(-1, padded)
    widths = (value, value, value, value, value, value, key, key, padded - lanes)
    scales = (SMALL_WEIGHT, FOX_OUT_WEIGHT, SMALL_WEIGHT, SMALL_WEIGHT, QUERY_WEIGHT)
    scales += (SMALL_WEIGHT, SMALL_WEIGHT, SMALL_WEIGHT, 1.0)
    forth = jnp.concatenate([jnp.full((w,), s, f32) for w, s in zip(widths, scales)])
    weights = lax.all_gather(
        (packed.astype(f32) * forth).astype(f16), "sp_0", axis=0, tiled=True
    )
    back = 1.0 / forth
    out_weight = (weights[:, : 2 * value].astype(f32) * back[: 2 * value]).astype(bf16)
    in_weight = (
        weights[:, 2 * value : lanes].astype(f32) * back[2 * value : lanes]
    ).astype(bf16)

    *parts, payload = kernel(
        lambda *refs: project_kernel(*refs, key=key, cores=cores),
        (
            jax.ShapeDtypeStruct((chunk, 2 * value), bf16),
            jax.ShapeDtypeStruct((chunk, value), bf16),
            jax.ShapeDtypeStruct((chunk, key), bf16),
            jax.ShapeDtypeStruct((chunk, key), bf16),
            jax.ShapeDtypeStruct((chunk + key, 2 * value), f32),
        ),
        [SMEM, SMEM, VMEM, VMEM, VMEM],
        20,
    )(place, ret_decay, wide, norm_gain.reshape(tp, 1, width), in_weight)

    sent = jnp.broadcast_to(out_weight[None], (cores * tp, *out_weight.shape))
    out_weights = lax.all_to_all(sent, CHIP, 0, 0, tiled=True)

    gathered = lax.all_gather(payload.astype(f16), "sp_0", axis=0, tiled=False)
    gathered = gathered.astype(f32).astype(bf16)

    mix = kernel(
        lambda *refs: mix_kernel(*refs, key=key),
        jax.ShapeDtypeStruct((chunk, 2 * value), bf16),
        [SMEM, SMEM] + [VMEM] * 8,
        24,
    )(
        place,
        ret_decay,
        *parts,
        gathered,
        fox_gates.T.reshape(cores, chips, 1, chunk),
        ret_state,
        head_norm_gain.reshape(cores, 1, value),
    )

    final = rows // tp
    mixes = lax.all_to_all(mix.reshape(cores * tp, final, -1), CHIP, 0, 0, tiled=True)
    return kernel(
        lambda *refs: output_kernel(*refs, cores=cores),
        jax.ShapeDtypeStruct((final, out_weight.shape[0]), bf16),
        [VMEM, VMEM],
        16,
    )(mixes, out_weights)


def solution(mesh):
    torus = Mesh(
        mesh.devices.reshape(mesh.shape["grp"], mesh.shape["sp"] // 2, 2, mesh.shape["tp"]),
        ("grp", "sp_0", "sp_1", "tp"),
    )
    return jax.shard_map(
        layer,
        mesh=torus,
        in_specs=(
            P(GRP_SP, "tp"),
            P(),
            P(SP, "tp"),
            P(SP, "tp"),
            P(SP, "tp"),
            P(SP, "tp"),
            P(SP, "tp"),
            P(SP, "tp"),
            P("tp"),
            P(("grp", "tp"), None, None),
            P("tp"),
            P("grp", "tp"),
            P("tp", SP),
            P("tp", SP),
        ),
        out_specs=P(GRP_SP_TP, None),
        check_vma=False,
    )
```

time: 263 us -> 281 us (1.068)
  blocking collectives: 215 us -> 241 us
  other arithmetic: 14.1 us -> 3.31 us
  Pallas kernels: 0.92 us -> 9.01 us
  local copies, waits for them, and re-layouts: 14.8 us -> 7.82 us
  matrix products: 6.09 us -> 0 us
  starting transfers between devices: 8.49 us -> 12.9 us
  waiting for transfers between devices: 0.72 us -> 4.43 us
    all_to_all x2 -> x1, blocking collectives: 23.2 us -> 51.8 us  [layer(): out_weights = lax.all_to_all(sent, CHIP, 0, 0, tiled=True)]
    all_to_all x1 -> x3, starting transfers between devices: 4.59 us -> 12.9 us  [the longest x1 4.79 us: layer(): wide = lax.all_to_all(sent, CHIP, 0, 0, tiled=True)]
    pallas_call x1 -> x4, Pallas kernels: 0.92 us -> 9.01 us  [the longest x1 2.79 us: layer(): kernel(lambda *refs: mix_kernel(*refs, key=key), jax.ShapeDtypeStruct((ch...]
    dot_general x6 -> x0, matrix products: 6.09 us -> none  [the longest x1 2.52 us: local(): inner = jnp.dot(near, ret_value.astype(f32), preferred_element_type=f32)]
    another operation x8 -> x1, other arithmetic: 5.62 us -> 0.08 us  [layer(): place = jnp.stack([chip, core]).astype(jnp.int32)]
    all_to_all x1 -> x3, waiting for transfers between devices: 0.01 us -> 4.43 us  [the longest x1 4.42 us: layer(): lax.all_to_all(mix.reshape(cores * tp, final, -1), CHIP, 0, 0, tiled=True)]
    ppermute x2 -> x0, starting transfers between devices: 3.9 us -> none  [the longest x1 1.95 us: local(): out_other = lax.ppermute(out_own, 'sp_1', swap)]
  transfers between devices with their start and end apart: 3 -> 3, of which waited for: 1 -> 1; matrix products, arithmetic and copies ran while one was open for 8% -> 2% of each run, Pallas kernels for 0% -> 0%
where the time goes in v2:
time: 281 us; the launch traced here: 279 us
  blocking collectives  241 us (86%)
  starting transfers between devices  12.9 us (5%)
  Pallas kernels  9.01 us (3%)
  local copies, waits for them, and re-layouts  7.82 us (3%)
  waiting for transfers between devices  4.43 us (2%)
  other arithmetic  3.31 us (1%)
    all_gather x1, blocking collectives, layer(): lax.all_gather((packed.astype(f32) * forth).astype(f16), 'sp_0', axis=0,...  109 us
    all_gather x1, blocking collectives, layer(): gathered = lax.all_gather(payload.astype(f16), 'sp_0', axis=0, tiled=False)  80.6 us
    all_to_all x1, blocking collectives, layer(): out_weights = lax.all_to_all(sent, CHIP, 0, 0, tiled=True)  51.8 us
  transfers between devices with their start and end apart: 3, of which 1 were waited for; matrix products, arithmetic and copies ran while one was open for 2% of the time, Pallas kernels for 0%

profile of v2, /device:TPU:40, one launch (start us, length us, event | category | flops | bytes accessed | tf_op | source)
XLA Modules:
  0.0 278.8 jit_solution(195419995952896912)
XLA Ops:
  0.0 1.5 pack.1
  1.5 3.3 %all-to-all-start.1 = ((bf16[2,32,512]{2,1,0:T(8,128)(2,1)}), bf16[2,32,512]{2,1,0:T(8,128)(2,1)S(1)}, u32[]{:S(2)}, u32[]{:S(2)}) async-start(bf16[2,32,512]{2,1,0:T(8,128)(2,1)} %pack.1), calls=%async_computation.1 | async-start | bytes 131072 | tf_op jit(solution)/shard_map/all_to_all | solution.py:221
  4.9 1.1 reshape.18.refs_7_
  6.0 0.7 reshape.19
  6.7 0.0 copy-start.5
  6.7 0.0 all-to-all-done.1
  6.7 2.5 broadcast_in_dim.4
  9.2 0.0 copy-start.6
  9.2 4.8 %all-to-all-start = ((bf16[8,256,512]{2,1,0:T(8,128)(2,1)}), bf16[8,256,512]{2,1,0:T(8,128)(2,1)S(1)}, u32[]{:S(2)}, u32[]{:S(2)}) async-start(bf16[8,256,512]{2,1,0:T(8,128)(2,1)} %broadcast_in_dim.4), calls=%async_computation | async-start | bytes 4194304 | tf_op jit(solution)/shard_map/all_to_all | solution.py:196
  14.0 0.0 copy-start.2
  14.0 0.0 copy-start.3
  14.0 0.1 pad_add_fusion.refs_0_
  14.1 0.0 copy-done.5
  14.1 108.9 %all-gather.3 = f16[2048,512]{1,0:T(8,128)(2,1)S(1)} all-gather(f16[64,512]{1,0:T(8,128)(2,1)S(1)} %fusion), channel_id=1, replica_groups=mesh['grp'=2,'sp_0'=32,'sp_1'=2,'tp'=4] {'sp_0'}, dimensions={0}, use_global_device_ids=true | all-gather | bytes 2162688 | tf_op jit(solution)/shard_map/all_gather | solution.py:226
  123.0 0.0 copy-start.4
  123.0 1.3 copy-done.4
  124.4 0.0 copy-done.6
  124.4 1.5 multiply_convert_fusion.refs_4_
  125.9 0.0 all-to-all-done.refs_2_
  125.9 0.0 copy-done.2
  125.9 0.0 copy-done.3
  125.9 0.0 copy-start
  125.9 1.4 copy-done
  127.3 2.4 shard_map.136
  129.8 80.6 %all-gather.4 = f16[17408,128]{1,0:T(8,128)(2,1)S(1)} all-gather(f16[544,128]{1,0:T(8,128)(2,1)S(1)} %convert_element_type.35), channel_id=2, replica_groups=mesh['grp'=2,'sp_0'=32,'sp_1'=2,'tp'=4] {'sp_0'}, dimensions={0}, use_global_device_ids=true | all-gather | bytes 4595712 | tf_op jit(solution)/shard_map/all_gather | solution.py:251
  210.3 0.0 copy-start.1
  210.3 0.5 convert_convert_fusion
  210.9 0.0 copy-start.7
  210.9 0.2 copy-done.1
  211.1 2.8 %shard_map.137 = bf16[512,128]{1,0:T(8,128)(2,1)} custom-call(s32[2]{0:T(128)S(1)} %pad_add_fusion.refs_0_, f32[2]{0:T(128)S(1)} %copy-done.3, bf16[512,128]{1,0:T(8,128)(2,1)S(1)} %get-tuple-element.10.refs_2_, bf16[512,64]{1,0:T(8,128)(2,1)S(1)} %get-tuple-element.11.refs_3_, bf16[512,32]{1,0:T(8,128)(2,1)S(1)} %get-tuple-element.12.refs_4_, ...), custom_call_target="tpu_custom_call" | custom-call | tf_op jit(solution)/shard_map/pallas_call | solution.py:254
  213.9 4.7 %all-to-all-start.2 = ((bf16[8,64,128]{2,1,0:T(8,128)(2,1)}), bf16[8,64,128]{2,1,0:T(8,128)(2,1)S(1)}, u32[]{:S(2)}, u32[]{:S(2)}) async-start(bf16[8,64,128]{2,1,0:T(8,128)(2,1)} %bitcast.9), calls=%async_computation.2 | async-start | bytes 262144 | tf_op jit(solution)/shard_map/all_to_all | solution.py:270
  218.6 0.0 copy-done.7
  218.6 1.1 multiply_convert_fusion.1
  219.8 4.4 %all-to-all-done.2.refs_0_ = bf16[8,64,128]{2,1,0:T(8,128)(2,1)S(1)} async-done(((bf16[8,64,128]{2,1,0:T(8,128)(2,1)}), bf16[8,64,128]{2,1,0:T(8,128)(2,1)S(1)}, u32[]{:S(2)}, u32[]{:S(2)}) %all-to-all-start.2) | async-done | bytes 131104 | tf_op jit(solution)/shard_map/all_to_all | solution.py:270
  224.2 0.5 broadcast_in_dim.5
  224.7 51.8 %all_to_all.20.refs_1_ = bf16[8,2048,128]{2,1,0:T(8,128)(2,1)S(1)} all-to-all(bf16[8,2048,128]{2,1,0:T(8,128)(2,1)S(1)} %broadcast_in_dim.5), channel_id=1, replica_groups=mesh['grp'=2,'sp_0'=32,'sp_1'=2,'tp'=4] {'sp_1','tp'}, dimensions={0} | all-to-all | bytes 8388608 | tf_op jit(solution)/shard_map/all_to_all | solution.py:249
  276.5 2.2 shard_map.138
  (2 shorter events, 0.1 us)
Async XLA Ops:
  1.5 5.2 %all-to-all-start.1 = ((bf16[2,32,512]{2,1,0:T(8,128)(2,1)}), bf16[2,32,512]{2,1,0:T(8,128)(2,1)S(1)}, u32[]{:S(2)}, u32[]{:S(2)}) async-start(bf16[2,32,512]{2,1,0:T(8,128)(2,1)} %pack.1), calls=%async_computation.1 | async-start | bytes 131072 | tf_op jit(solution)/shard_map/all_to_all | solution.py:221
  6.7 7.4 %copy-start.5 = (f32[512]{0:T(512)S(1)}, f32[512]{0:T(512)}, u32[]{:S(2)}) copy-start(f32[512]{0:T(512)} %constant.18.clone.1) | copy-start | bytes 6148
  9.2 115.2 %copy-start.6 = (f32[320]{0:T(512)S(1)}, f32[320]{0:T(512)}, u32[]{:S(2)}) copy-start(f32[320]{0:T(512)} %constant.19.clone.1) | copy-start | bytes 3844
  9.2 116.7 %all-to-all-start = ((bf16[8,256,512]{2,1,0:T(8,128)(2,1)}), bf16[8,256,512]{2,1,0:T(8,128)(2,1)S(1)}, u32[]{:S(2)}, u32[]{:S(2)}) async-start(bf16[8,256,512]{2,1,0:T(8,128)(2,1)} %broadcast_in_dim.4), calls=%async_computation | async-start | bytes 4194304 | tf_op jit(solution)/shard_map/all_to_all | solution.py:196
  14.0 111.9 %copy-start.2 = (f32[2048]{0:T(1024)S(1)}, f32[2048]{0:T(1024)}, u32[]{:S(2)}) copy-start(f32[2048]{0:T(1024)} %param.15) | copy-start | bytes 24580
  14.0 111.9 %copy-start.3 = (f32[2]{0:T(128)S(1)}, f32[2]{0:T(128)}, u32[]{:S(2)}) copy-start(f32[2]{0:T(128)} %refs_1_.3) | copy-start | bytes 28
  123.0 1.3 copy-start.4
  125.9 1.4 copy-start
  210.3 0.8 copy-start.1
  210.9 7.8 %copy-start.7 = (f32[128]{0:T(128)S(1)}, f32[128]{0:T(128)}, u32[]{:S(2)}) copy-start(f32[128]{0:T(128)} %constant.20.clone.1) | copy-start | bytes 1540
  213.9 10.3 %all-to-all-start.2 = ((bf16[8,64,128]{2,1,0:T(8,128)(2,1)}), bf16[8,64,128]{2,1,0:T(8,128)(2,1)S(1)}, u32[]{:S(2)}, u32[]{:S(2)}) async-start(bf16[8,64,128]{2,1,0:T(8,128)(2,1)} %bitcast.9), calls=%async_computation.2 | async-start | bytes 262144 | tf_op jit(solution)/shard_map/all_to_all | solution.py:270

commit v3 on v2

--- a/solution.py
+++ b/solution.py
@@ -25,6 +25,7 @@
 
 VMEM = pl.BlockSpec(memory_space=pltpu.VMEM)
 SMEM = pl.BlockSpec(memory_space=pltpu.SMEM)
+HBM = pl.BlockSpec(memory_space=pltpu.HBM)
 NT = (((1,), (1,)), ((), ()))
 TN = (((0,), (0,)), ((), ()))
 
@@ -42,9 +43,18 @@
     return lax.broadcasted_iota(jnp.int32, (count, 1), 0).astype(jnp.float32)
 
 
-def pack_kernel(out_ret, out_fox, fk, fv, fq, rv, rk, rq, packed):
+def copies(source, target, signals):
+    return [
+        pltpu.make_async_copy(source, target.at[k], signals.at[k]) for k in range(target.shape[0])
+    ]
+
+
+def pack_kernel(tokens, out_ret, out_fox, fk, fv, fq, rv, rk, rq, packed, sent, signals):
     f32 = jnp.float32
     heads = packed.shape[0]
+    started = copies(tokens, sent, signals)
+    for copy in started:
+        copy.start()
 
     def columns(ref, h):
         size = ref.shape[1] // heads
@@ -56,24 +66,54 @@
         blank = packed.shape[2] - joined.shape[1]
         joined = jnp.concatenate([joined, jnp.zeros((joined.shape[0], blank), f32)], axis=1)
         packed[h] = joined.astype(packed.dtype)
-
-
-def project_kernel(place, decays, tokens, gains, weights, query, values, keys, queries, payload, *, key, cores):
+    for copy in started:
+        copy.wait()
+
+
+def project_kernel(
+    place,
+    decays,
+    tokens,
+    gains,
+    stored,
+    back,
+    query,
+    values,
+    keys,
+    queries,
+    payload,
+    sent,
+    weights,
+    arrived,
+    signals,
+    *,
+    key,
+    cores,
+):
     f32, bf16 = jnp.float32, jnp.bfloat16
     rows, width = tokens.shape[1:]
     parts, value = tokens.shape[0] // cores, 2 * key
+    first, last = 2 * value, 6 * value + 2 * key
+    reading = pltpu.make_async_copy(stored, weights, arrived)
+    reading.start()
+    factors = []
     for c in range(cores):
         square = jnp.zeros((rows, 1), f32)
         for k in range(parts):
             x = tokens[c * parts + k].astype(f32)
             square = square + jnp.sum(x * x, axis=1, keepdims=True)
-        factor = lax.rsqrt(square * (1.0 / (parts * width)) + EPSILON)
-        total = jnp.zeros((rows, weights.shape[1]), f32)
+        factors.append(lax.rsqrt(square * (1.0 / (parts * width)) + EPSILON))
+    reading.wait()
+    started = copies(weights.at[:, :first], sent, signals)
+    for copy in started:
+        copy.start()
+    for c in range(cores):
+        total = jnp.zeros((rows, last - first), f32)
         for k in range(parts):
             x = tokens[c * parts + k].astype(f32)
-            normed = (x * factor * gains[k]).astype(bf16)
-            total = total + dot(normed, weights[k * width : (k + 1) * width, :])
-        total = total.astype(bf16)
+            normed = (x * factors[c] * gains[k]).astype(bf16)
+            total = total + dot(normed, weights[k * width : (k + 1) * width, first:last])
+        total = (total * back[:, first:last]).astype(bf16)
         at = slice(c * rows, (c + 1) * rows)
         payload[at, :] = total[:, : 2 * value].astype(f32) * KEY_VALUE
         lane = lax.broadcasted_iota(jnp.int32, (rows, 2 * value), 1)
@@ -88,6 +128,8 @@
     summary = (dot(high, values[...], TN) + dot(low, values[...], TN)) * STATE
     high = summary.astype(bf16).astype(f32)
     payload[chunk:, :] = jnp.concatenate([high, (summary - high) * STATE_LOW], axis=1)
+    for copy in started:
+        copy.wait()
 
 
 def mix_kernel(place, decays, query, values, keys, queries, gathered, gates, state, gains, mix, *, key):
@@ -97,11 +139,16 @@
     decay = decays[head]
     attending = query[...]
     scale = value ** (-0.5) * LOG2E / KEY_VALUE
-    base = jnp.max(gates[head, own], axis=1, keepdims=True)
+
+    def gates_of(j):
+        pair = gates[:, pl.ds(pl.multiple_of(j * chunk, chunk), chunk)]
+        return jnp.where(head == 0, pair[:1], pair[1:])
+
+    base = jnp.max(gates_of(own), axis=1, keepdims=True)
 
     def logits_of(j):
         pairs = gathered[j, :chunk, :]
-        return dot(attending, pairs, NT) * scale - (gates[head, j] - base) * LOG2E, pairs
+        return dot(attending, pairs, NT) * scale - (gates_of(j) - base) * LOG2E, pairs
 
     row = lax.broadcasted_iota(jnp.int32, (chunk, chunk), 0)
     col = lax.broadcasted_iota(jnp.int32, (chunk, chunk), 1)
@@ -142,8 +189,10 @@
     raw = dot(near.astype(bf16), values[...]) + carried * jnp.exp((column_of(chunk) + 1.0) * decay)
     center = raw - jnp.mean(raw, axis=1, keepdims=True)
     variance = jnp.mean(center * center, axis=1, keepdims=True)
-    ret = center * lax.rsqrt(variance + EPSILON) * gains[head]
-    mix[...] = jnp.concatenate([ret, fox], axis=1).astype(bf16)
+    gain = jnp.where(head == 0, gains[:, :value], gains[:, value:])
+    ret = center * lax.rsqrt(variance + EPSILON) * gain
+    joined = [ret * (1.0 / SMALL_WEIGHT), fox * (1.0 / FOX_OUT_WEIGHT)]
+    mix[...] = jnp.concatenate(joined, axis=1).astype(bf16)
 
 
 def output_kernel(mixes, weights, out, *, cores):
@@ -158,14 +207,17 @@
 
 
 def kernel(body, out_shape, in_specs, limit):
-    many = isinstance(out_shape, tuple)
     return pl.pallas_call(
         body,
         out_shape=out_shape,
         in_specs=in_specs,
-        out_specs=(VMEM,) * len(out_shape) if many else VMEM,
+        out_specs=VMEM,
         compiler_params=pltpu.CompilerParams(vmem_limit_bytes=limit * MIB),
     )
+
+
+def whole(*shape):
+    return pl.BlockSpec(shape, lambda i: (0,) * len(shape))
 
 
 def layer(
@@ -186,29 +238,30 @@
 ):
     f32, bf16, f16 = jnp.float32, jnp.bfloat16, jnp.float16
     chip, core = lax.axis_index("sp_0"), lax.axis_index("sp_1")
-    chips, cores, tp = (lax.axis_size(a) for a in ("sp_0", "sp_1", "tp"))
+    cores, tp = lax.axis_size("sp_1"), lax.axis_size("tp")
     rows, width = tokens.shape
     chunk = rows * cores
     key, value = ret_query_weight.shape[1] // cores, ret_value_weight.shape[1] // cores
     place = jnp.stack([chip, core]).astype(jnp.int32)
 
-    sent = jnp.broadcast_to(tokens[None], (cores * tp, rows, width))
-    wide = lax.all_to_all(sent, CHIP, 0, 0, tiled=True)
-
+    peers = cores * tp
     shard = fox_key_weight.shape[0]
-    lanes = 2 * value + 4 * value + 2 * key
+    lanes = 6 * value + 2 * key
     padded = lanes + -lanes % 128
-    packed = pl.pallas_call(
+    packed, sent = pl.pallas_call(
         pack_kernel,
-        out_shape=jax.ShapeDtypeStruct((cores, shard, padded), bf16),
+        out_shape=(
+            jax.ShapeDtypeStruct((cores, shard, padded), bf16),
+            jax.ShapeDtypeStruct((peers, rows, width), bf16),
+        ),
         grid=(1,),
-        in_specs=[
-            pl.BlockSpec((shard, size * cores), lambda i: (0, 0))
-            for size in (value,) * 6 + (key,) * 2
-        ],
-        out_specs=pl.BlockSpec((cores, shard, padded), lambda i: (0, 0, 0)),
+        in_specs=[HBM]
+        + [whole(shard, size * cores) for size in (value,) * 6 + (key,) * 2],
+        out_specs=(whole(cores, shard, padded), HBM),
+        scratch_shapes=[pltpu.SemaphoreType.DMA((peers,))],
         name="pack",
     )(
+        tokens,
         ret_out_weight.T,
         fox_out_weight.T,
         fox_key_weight,
@@ -218,6 +271,8 @@
         ret_key_weight,
         ret_query_weight,
     )
+    wide = lax.all_to_all(sent, CHIP, 0, 0, tiled=True)
+
     packed = lax.all_to_all(packed, "sp_1", 0, 0, tiled=True).reshape(-1, padded)
     widths = (value, value, value, value, value, value, key, key, padded - lanes)
     scales = (SMALL_WEIGHT, FOX_OUT_WEIGHT, SMALL_WEIGHT, SMALL_WEIGHT, QUERY_WEIGHT)
@@ -226,26 +281,28 @@
     weights = lax.all_gather(
         (packed.astype(f32) * forth).astype(f16), "sp_0", axis=0, tiled=True
     )
-    back = 1.0 / forth
-    out_weight = (weights[:, : 2 * value].astype(f32) * back[: 2 * value]).astype(bf16)
-    in_weight = (
-        weights[:, 2 * value : lanes].astype(f32) * back[2 * value : lanes]
-    ).astype(bf16)
-
-    *parts, payload = kernel(
+    weights = weights.astype(f32).astype(bf16)
+    *parts, payload, sent = pl.pallas_call(
         lambda *refs: project_kernel(*refs, key=key, cores=cores),
-        (
+        out_shape=(
             jax.ShapeDtypeStruct((chunk, 2 * value), bf16),
             jax.ShapeDtypeStruct((chunk, value), bf16),
             jax.ShapeDtypeStruct((chunk, key), bf16),
             jax.ShapeDtypeStruct((chunk, key), bf16),
             jax.ShapeDtypeStruct((chunk + key, 2 * value), f32),
+            jax.ShapeDtypeStruct((peers, weights.shape[0], 2 * value), bf16),
         ),
-        [SMEM, SMEM, VMEM, VMEM, VMEM],
-        20,
-    )(place, ret_decay, wide, norm_gain.reshape(tp, 1, width), in_weight)
-
-    sent = jnp.broadcast_to(out_weight[None], (cores * tp, *out_weight.shape))
+        in_specs=[SMEM, SMEM, VMEM, VMEM, HBM, VMEM],
+        out_specs=(VMEM,) * 5 + (HBM,),
+        scratch_shapes=[
+            pltpu.VMEM(weights.shape, bf16),
+            pltpu.SemaphoreType.DMA,
+            pltpu.SemaphoreType.DMA((peers,)),
+        ],
+        compiler_params=pltpu.CompilerParams(vmem_limit_bytes=20 * MIB),
+        name="project",
+    )(place, ret_decay, wide, norm_gain.reshape(tp, 1, width), weights, (1.0 / forth)[None])
+
     out_weights = lax.all_to_all(sent, CHIP, 0, 0, tiled=True)
 
     gathered = lax.all_gather(payload.astype(f16), "sp_0", axis=0, tiled=False)
@@ -261,18 +318,25 @@
         ret_decay,
         *parts,
         gathered,
-        fox_gates.T.reshape(cores, chips, 1, chunk),
+        fox_gates.T,
         ret_state,
-        head_norm_gain.reshape(cores, 1, value),
+        head_norm_gain[None],
     )
 
     final = rows // tp
     mixes = lax.all_to_all(mix.reshape(cores * tp, final, -1), CHIP, 0, 0, tiled=True)
-    return kernel(
+    features = out_weights.shape[1]
+    block = features // 4
+    return pl.pallas_call(
         lambda *refs: output_kernel(*refs, cores=cores),
-        jax.ShapeDtypeStruct((final, out_weight.shape[0]), bf16),
-        [VMEM, VMEM],
-        16,
+        out_shape=jax.ShapeDtypeStruct((final, features), bf16),
+        grid=(features // block,),
+        in_specs=[
+            whole(*mixes.shape),
+            pl.BlockSpec((peers, block, 2 * value), lambda i: (0, i, 0)),
+        ],
+        out_specs=pl.BlockSpec((final, block), lambda i: (0, i)),
+        name="output",
     )(mixes, out_weights)
 
 

time: 281 us -> 345 us (1.23)
  Pallas kernels: 9.01 us -> 76.7 us
  blocking collectives: 241 us -> 252 us
  local copies, waits for them, and re-layouts: 7.82 us -> 1.97 us
  starting transfers between devices: 12.9 us -> 7.92 us
    pallas_call x3, Pallas kernels: 6.22 us -> 74.5 us  [the longest x1 66.2 us: layer(): pl.pallas_call(pack_kernel, out_shape=(jax.ShapeDtypeStruct((cores, shard...]
    all_to_all x0 -> x1, blocking collectives: none -> 10.5 us  [layer(): lax.all_to_all(mix.reshape(cores * tp, final, -1), CHIP, 0, 0, tiled=True)]
    all_to_all x1 -> x0, starting transfers between devices: 4.74 us -> none  [layer(): lax.all_to_all(mix.reshape(cores * tp, final, -1), CHIP, 0, 0, tiled=True)]
    all_to_all x1 -> x0, waiting for transfers between devices: 4.42 us -> none  [layer(): lax.all_to_all(mix.reshape(cores * tp, final, -1), CHIP, 0, 0, tiled=True)]
  transfers between devices with their start and end apart: 3 -> 2, of which waited for: 1 -> 1; matrix products, arithmetic and copies ran while one was open for 2% -> 1% of each run, Pallas kernels for 0% -> 0%
where the time goes in v3:
time: 345 us; the launch traced here: 343 us
  blocking collectives  252 us (73%)
  Pallas kernels  76.7 us (22%)
  starting transfers between devices  7.92 us (2%)
    all_gather x1, blocking collectives, layer(): lax.all_gather((packed.astype(f32) * forth).astype(f16), 'sp_0', axis=0,...  109 us
    all_gather x1, blocking collectives, layer(): gathered = lax.all_gather(payload.astype(f16), 'sp_0', axis=0, tiled=False)  80.5 us
    pallas_call x1, Pallas kernels, layer(): pl.pallas_call(pack_kernel, out_shape=(jax.ShapeDtypeStruct((cores, shard...  66.2 us
    all_to_all x1, blocking collectives, layer(): out_weights = lax.all_to_all(sent, CHIP, 0, 0, tiled=True)  52.4 us
    all_to_all x1, blocking collectives, layer(): lax.all_to_all(mix.reshape(cores * tp, final, -1), CHIP, 0, 0, tiled=True)  10.5 us
  transfers between devices with their start and end apart: 2, of which 1 were waited for; matrix products, arithmetic and copies ran while one was open for 1% of the time, Pallas kernels for 0%

profile of v3, /device:TPU:40, one launch (start us, length us, event | category | flops | bytes accessed | tf_op | source)
XLA Modules:
  0.0 342.7 jit_solution(5521307778851005773)
XLA Ops:
  0.0 0.0 copy-start.7
  0.0 66.2 %pack.1 = (bf16[2,32,512]{2,1,0:T(8,128)(2,1)}, bf16[8,256,512]{2,1,0:T(8,128)(2,1)}) custom-call(bf16[256,512]{1,0:T(8,128)(2,1)} %tokens.1, bf16[32,128]{1,0:T(8,128)(2,1)} %bitcast.17, bf16[32,128]{1,0:T(8,128)(2,1)} %bitcast.18, bf16[32,128]{1,0:T(8,128)(2,1)} %fk.1, bf16[32,128]{1,0:T(8,128)(2,1)} %fv.1, bf16[32,128]{1,0:T(8,128)(2,1)} %fq.1, ...), custom_call_target="tpu_custom_call" | custom-call | tf_op jit(solution)/shard_map/pack/pallas_call | solution.py:251
  66.2 3.3 all-to-all-start.1
  69.5 1.4 all-to-all-done.1
  70.9 4.6 %all-to-all-start = ((bf16[8,256,512]{2,1,0:T(8,128)(2,1)}), bf16[8,256,512]{2,1,0:T(8,128)(2,1)S(1)}, u32[]{:S(2)}, u32[]{:S(2)}) async-start(bf16[8,256,512]{2,1,0:T(8,128)(2,1)} %get-tuple-element.13), calls=%async_computation | async-start | bytes 4194304 | tf_op jit(solution)/shard_map/all_to_all | solution.py:274
  75.5 0.0 copy-start.3
  75.5 0.0 copy-start.4
  75.5 0.0 copy-start.5
  75.5 0.1 pad_add_fusion.refs_0_
  75.6 0.0 copy-done.7
  75.6 108.9 %all-gather.3 = f16[2048,512]{1,0:T(8,128)(2,1)S(1)} all-gather(f16[64,512]{1,0:T(8,128)(2,1)S(1)} %fusion), channel_id=1, replica_groups=mesh['grp'=2,'sp_0'=32,'sp_1'=2,'tp'=4] {'sp_0'}, dimensions={0}, use_global_device_ids=true | all-gather | bytes 2162688 | tf_op jit(solution)/shard_map/all_gather | solution.py:281
  184.5 1.7 convert_convert_fusion.1.refs_4_
  186.2 0.0 all-to-all-done.refs_2_
  186.3 0.0 copy-done.3
  186.3 0.0 copy-done.4
  186.3 0.0 copy-done.5
  186.3 0.0 copy-start
  186.3 1.6 copy-done
  187.9 3.6 %project.1 = (bf16[512,128]{1,0:T(8,128)(2,1)S(1)}, bf16[512,64]{1,0:T(8,128)(2,1)S(1)}, bf16[512,32]{1,0:T(8,128)(2,1)S(1)}, bf16[512,32]{1,0:T(8,128)(2,1)S(1)...) custom-call(s32[2]{0:T(128)S(1)} %pad_add_fusion.refs_0_, f32[2]{0:T(128)S(1)} %copy-done.5, ...), custom_call_target="tpu_custom_call" | custom-call | tf_op jit(solution)/shard_map/project/pallas_call | solution.py:285
  191.5 80.5 %all-gather.4 = f16[17408,128]{1,0:T(8,128)(2,1)S(1)} all-gather(f16[544,128]{1,0:T(8,128)(2,1)S(1)} %convert_element_type.29), channel_id=2, replica_groups=mesh['grp'=2,'sp_0'=32,'sp_1'=2,'tp'=4] {'sp_0'}, dimensions={0}, use_global_device_ids=true | all-gather | bytes 4595712 | tf_op jit(solution)/shard_map/all_gather | solution.py:308
  272.0 0.0 copy-start.1
  272.0 0.0 copy-start.2
  272.0 0.0 copy-start.6
  272.0 0.5 convert_convert_fusion
  272.5 0.4 copy-done.1
  272.9 0.0 copy-done.2
  272.9 0.0 copy-done.6
  272.9 2.2 shard_map.136
  275.1 10.5 %all_to_all.20.refs_0_ = bf16[8,64,128]{2,1,0:T(8,128)(2,1)} all-to-all(bf16[8,64,128]{2,1,0:T(8,128)(2,1)S(1)} %bitcast.13), channel_id=1, replica_groups=mesh['grp'=2,'sp_0'=32,'sp_1'=2,'tp'=4] {'sp_1','tp'}, dimensions={0} | all-to-all | bytes 262144 | tf_op jit(solution)/shard_map/all_to_all | solution.py:327
  285.6 52.4 %all_to_all.21.refs_1_ = bf16[8,2048,128]{2,1,0:T(8,128)(2,1)} all-to-all(bf16[8,2048,128]{2,1,0:T(8,128)(2,1)S(1)} %get-tuple-element.20), channel_id=1, replica_groups=mesh['grp'=2,'sp_0'=32,'sp_1'=2,'tp'=4] {'sp_1','tp'}, dimensions={0} | all-to-all | bytes 8388608 | tf_op jit(solution)/shard_map/all_to_all | solution.py:306
  337.9 4.8 %output.1 = bf16[64,2048]{1,0:T(8,128)(2,1)} custom-call(bf16[8,64,128]{2,1,0:T(8,128)(2,1)} %all_to_all.20.refs_0_, bf16[8,2048,128]{2,1,0:T(8,128)(2,1)} %all_to_all.21.refs_1_), custom_call_target="tpu_custom_call" | custom-call | tf_op jit(solution)/shard_map/output/pallas_call | solution.py:330
  (2 shorter events, 0.0 us)
Async XLA Ops:
  0.0 75.6 %copy-start.7 = (f32[512]{0:T(512)S(1)}, f32[512]{0:T(512)}, u32[]{:S(2)}) copy-start(f32[512]{0:T(512)} %constant.15.clone.1) | copy-start | bytes 6148
  66.2 4.7 %all-to-all-start.1 = ((bf16[2,32,512]{2,1,0:T(8,128)(2,1)}), bf16[2,32,512]{2,1,0:T(8,128)(2,1)S(1)}, u32[]{:S(2)}, u32[]{:S(2)}) async-start(bf16[2,32,512]{2,1,0:T(8,128)(2,1)} %get-tuple-element.14), calls=%async_computation.1 | async-start | bytes 131072 | tf_op jit(solution)/shard_map/all_to_all | solution.py:276
  70.9 115.4 %all-to-all-start = ((bf16[8,256,512]{2,1,0:T(8,128)(2,1)}), bf16[8,256,512]{2,1,0:T(8,128)(2,1)S(1)}, u32[]{:S(2)}, u32[]{:S(2)}) async-start(bf16[8,256,512]{2,1,0:T(8,128)(2,1)} %get-tuple-element.13), calls=%async_computation | async-start | bytes 4194304 | tf_op jit(solution)/shard_map/all_to_all | solution.py:274
  75.5 110.8 %copy-start.3 = (f32[2048]{0:T(1024)S(1)}, f32[2048]{0:T(1024)}, u32[]{:S(2)}) copy-start(f32[2048]{0:T(1024)} %param.15) | copy-start | bytes 24580
  75.5 110.8 %copy-start.4 = (f32[1,512]{1,0:T(1,128)S(1)}, f32[1,512]{1,0:T(1,128)}, u32[]{:S(2)}) copy-start(f32[1,512]{1,0:T(1,128)} %constant.16.clone.1.refs_5_) | copy-start | bytes 6148
  75.5 110.8 %copy-start.5 = (f32[2]{0:T(128)S(1)}, f32[2]{0:T(128)}, u32[]{:S(2)}) copy-start(f32[2]{0:T(128)} %refs_1_.3) | copy-start | bytes 28
  186.3 1.6 copy-start
  272.0 0.9 copy-start.1
  272.0 0.9 copy-start.2
  272.0 0.9 copy-start.6

commit v4 on v3

--- a/solution.py
+++ b/solution.py
@@ -49,9 +49,11 @@
     ]
 
 
-def pack_kernel(tokens, out_ret, out_fox, fk, fv, fq, rv, rk, rq, packed, sent, signals):
+def pack_kernel(
+    core, tokens, out_ret, out_fox, fk, fv, fq, rv, rk, rq, mine, theirs, sent, signals
+):
     f32 = jnp.float32
-    heads = packed.shape[0]
+    heads = 2
     started = copies(tokens, sent, signals)
     for copy in started:
         copy.start()
@@ -60,12 +62,17 @@
         size = ref.shape[1] // heads
         return ref[...].astype(f32)[:, h * size : (h + 1) * size]
 
+    both = []
     for h in range(heads):
         parts = [columns(ref, h) for ref in (out_ret, out_fox, fk, fv, fq, rv, rk, rq)]
         joined = jnp.concatenate(parts, axis=1)
-        blank = packed.shape[2] - joined.shape[1]
-        joined = jnp.concatenate([joined, jnp.zeros((joined.shape[0], blank), f32)], axis=1)
-        packed[h] = joined.astype(packed.dtype)
+        blank = mine.shape[1] - joined.shape[1]
+        both.append(jnp.concatenate([joined, jnp.zeros((joined.shape[0], blank), f32)], axis=1))
+    shard = both[0].shape[0]
+    for c in range(heads):
+        at = slice(c * shard, (c + 1) * shard)
+        mine[at, :] = jnp.where(core[0] == c, both[c], 0.0).astype(mine.dtype)
+        theirs[at, :] = jnp.where(core[0] == c, both[1 - c], 0.0).astype(theirs.dtype)
     for copy in started:
         copy.wait()
 
@@ -75,44 +82,35 @@
     decays,
     tokens,
     gains,
-    stored,
+    weights,
     back,
     query,
     values,
     keys,
     queries,
     payload,
-    sent,
-    weights,
-    arrived,
-    signals,
     *,
     key,
     cores,
 ):
     f32, bf16 = jnp.float32, jnp.bfloat16
-    rows, width = tokens.shape[1:]
-    parts, value = tokens.shape[0] // cores, 2 * key
+    width = tokens.shape[1]
+    parts, value = weights.shape[0], 2 * key
+    rows = tokens.shape[0] // (cores * parts)
     first, last = 2 * value, 6 * value + 2 * key
-    reading = pltpu.make_async_copy(stored, weights, arrived)
-    reading.start()
     factors = []
     for c in range(cores):
         square = jnp.zeros((rows, 1), f32)
         for k in range(parts):
-            x = tokens[c * parts + k].astype(f32)
+            x = tokens[(c * parts + k) * rows : (c * parts + k + 1) * rows, :].astype(f32)
             square = square + jnp.sum(x * x, axis=1, keepdims=True)
         factors.append(lax.rsqrt(square * (1.0 / (parts * width)) + EPSILON))
-    reading.wait()
-    started = copies(weights.at[:, :first], sent, signals)
-    for copy in started:
-        copy.start()
     for c in range(cores):
         total = jnp.zeros((rows, last - first), f32)
         for k in range(parts):
-            x = tokens[c * parts + k].astype(f32)
+            x = tokens[(c * parts + k) * rows : (c * parts + k + 1) * rows, :].astype(f32)
             normed = (x * factors[c] * gains[k]).astype(bf16)
-            total = total + dot(normed, weights[k * width : (k + 1) * width, first:last])
+            total = total + dot(normed, weights[k][:, first:last])
         total = (total * back[:, first:last]).astype(bf16)
         at = slice(c * rows, (c + 1) * rows)
         payload[at, :] = total[:, : 2 * value].astype(f32) * KEY_VALUE
@@ -128,8 +126,6 @@
     summary = (dot(high, values[...], TN) + dot(low, values[...], TN)) * STATE
     high = summary.astype(bf16).astype(f32)
     payload[chunk:, :] = jnp.concatenate([high, (summary - high) * STATE_LOW], axis=1)
-    for copy in started:
-        copy.wait()
 
 
 def mix_kernel(place, decays, query, values, keys, queries, gathered, gates, state, gains, mix, *, key):
@@ -246,21 +242,24 @@
 
     peers = cores * tp
     shard = fox_key_weight.shape[0]
+    chip_shard = shard * cores
     lanes = 6 * value + 2 * key
     padded = lanes + -lanes % 128
-    packed, sent = pl.pallas_call(
+    mine, theirs, sent = pl.pallas_call(
         pack_kernel,
         out_shape=(
-            jax.ShapeDtypeStruct((cores, shard, padded), bf16),
+            jax.ShapeDtypeStruct((chip_shard, padded), bf16),
+            jax.ShapeDtypeStruct((chip_shard, padded), bf16),
             jax.ShapeDtypeStruct((peers, rows, width), bf16),
         ),
         grid=(1,),
-        in_specs=[HBM]
+        in_specs=[SMEM, whole(rows, width)]
         + [whole(shard, size * cores) for size in (value,) * 6 + (key,) * 2],
-        out_specs=(whole(cores, shard, padded), HBM),
+        out_specs=(VMEM, VMEM, HBM),
         scratch_shapes=[pltpu.SemaphoreType.DMA((peers,))],
         name="pack",
     )(
+        place[1:],
         tokens,
         ret_out_weight.T,
         fox_out_weight.T,
@@ -273,16 +272,17 @@
     )
     wide = lax.all_to_all(sent, CHIP, 0, 0, tiled=True)
 
-    packed = lax.all_to_all(packed, "sp_1", 0, 0, tiled=True).reshape(-1, padded)
+    got = lax.ppermute(theirs, "sp_1", [(0, 1), (1, 0)])
+    packed = mine.astype(f32) + got.astype(f32)
     widths = (value, value, value, value, value, value, key, key, padded - lanes)
     scales = (SMALL_WEIGHT, FOX_OUT_WEIGHT, SMALL_WEIGHT, SMALL_WEIGHT, QUERY_WEIGHT)
     scales += (SMALL_WEIGHT, SMALL_WEIGHT, SMALL_WEIGHT, 1.0)
     forth = jnp.concatenate([jnp.full((w,), s, f32) for w, s in zip(widths, scales)])
     weights = lax.all_gather(
-        (packed.astype(f32) * forth).astype(f16), "sp_0", axis=0, tiled=True
+        (packed * forth).astype(f16), "sp_0", axis=0, tiled=True
     )
     weights = weights.astype(f32).astype(bf16)
-    *parts, payload, sent = pl.pallas_call(
+    *parts, payload = pl.pallas_call(
         lambda *refs: project_kernel(*refs, key=key, cores=cores),
         out_shape=(
             jax.ShapeDtypeStruct((chunk, 2 * value), bf16),
@@ -290,19 +290,21 @@
             jax.ShapeDtypeStruct((chunk, key), bf16),
             jax.ShapeDtypeStruct((chunk, key), bf16),
             jax.ShapeDtypeStruct((chunk + key, 2 * value), f32),
-            jax.ShapeDtypeStruct((peers, weights.shape[0], 2 * value), bf16),
         ),
-        in_specs=[SMEM, SMEM, VMEM, VMEM, HBM, VMEM],
-        out_specs=(VMEM,) * 5 + (HBM,),
-        scratch_shapes=[
-            pltpu.VMEM(weights.shape, bf16),
-            pltpu.SemaphoreType.DMA,
-            pltpu.SemaphoreType.DMA((peers,)),
-        ],
+        in_specs=[SMEM, SMEM] + [VMEM] * 4,
+        out_specs=(VMEM,) * 5,
         compiler_params=pltpu.CompilerParams(vmem_limit_bytes=20 * MIB),
         name="project",
-    )(place, ret_decay, wide, norm_gain.reshape(tp, 1, width), weights, (1.0 / forth)[None])
-
+    )(
+        place,
+        ret_decay,
+        wide.reshape(-1, width),
+        norm_gain.reshape(tp, 1, width),
+        weights.reshape(tp, width, padded),
+        (1.0 / forth)[None],
+    )
+
+    sent = jnp.broadcast_to(weights[None, :, : 2 * value], (peers, weights.shape[0], 2 * value))
     out_weights = lax.all_to_all(sent, CHIP, 0, 0, tiled=True)
 
     gathered = lax.all_gather(payload.astype(f16), "sp_0", axis=0, tiled=False)
@@ -325,18 +327,11 @@
 
     final = rows // tp
     mixes = lax.all_to_all(mix.reshape(cores * tp, final, -1), CHIP, 0, 0, tiled=True)
-    features = out_weights.shape[1]
-    block = features // 4
-    return pl.pallas_call(
+    return kernel(
         lambda *refs: output_kernel(*refs, cores=cores),
-        out_shape=jax.ShapeDtypeStruct((final, features), bf16),
-        grid=(features // block,),
-        in_specs=[
-            whole(*mixes.shape),
-            pl.BlockSpec((peers, block, 2 * value), lambda i: (0, i, 0)),
-        ],
-        out_specs=pl.BlockSpec((final, block), lambda i: (0, i)),
-        name="output",
+        jax.ShapeDtypeStruct((final, out_weights.shape[1]), bf16),
+        [VMEM, VMEM],
+        16,
     )(mixes, out_weights)
 
 

time: 345 us -> 276 us (0.80)
  Pallas kernels: 76.7 us -> 11.8 us
  blocking collectives: 252 us -> 242 us
  waiting for transfers between devices: 1.38 us -> 6.31 us
  starting transfers between devices: 7.92 us -> 11.4 us
    pallas_call x2, Pallas kernels: 70.9 us -> 5.31 us  [the longest x1 3.06 us: layer(): pl.pallas_call(pack_kernel, out_shape=(jax.ShapeDtypeStruct((chip_shard,...]
    all_to_all x1 -> x0, blocking collectives: 10.5 us -> none  [layer(): lax.all_to_all(mix.reshape(cores * tp, final, -1), CHIP, 0, 0, tiled=True)]
    all_to_all x1, waiting for transfers between devices: 1.38 us -> 5.51 us  [layer(): lax.all_to_all(mix.reshape(cores * tp, final, -1), CHIP, 0, 0, tiled=True)]
  transfers between devices with their start and end apart: 2 -> 3, of which waited for: 1 -> 2; matrix products, arithmetic and copies ran while one was open for 1% -> 0% of each run, Pallas kernels for 0% -> 0%
where the time goes in v4:
time: 276 us; the launch traced here: 274 us
  blocking collectives  242 us (88%)
  Pallas kernels  11.8 us (4%)
  starting transfers between devices  11.4 us (4%)
  waiting for transfers between devices  6.31 us (2%)
    all_gather x1, blocking collectives, layer(): lax.all_gather((packed * forth).astype(f16), 'sp_0', axis=0, tiled=True)  108 us
    all_gather x1, blocking collectives, layer(): gathered = lax.all_gather(payload.astype(f16), 'sp_0', axis=0, tiled=False)  82 us
    all_to_all x1, blocking collectives, layer(): out_weights = lax.all_to_all(sent, CHIP, 0, 0, tiled=True)  51.8 us
  transfers between devices with their start and end apart: 3, of which 2 were waited for; matrix products, arithmetic and copies ran while one was open for 0% of the time, Pallas kernels for 0%

profile of v4, /device:TPU:40, one launch (start us, length us, event | category | flops | bytes accessed | tf_op | source)
XLA Modules:
  0.0 273.8 jit_solution(4994140099836172207)
XLA Ops:
  0.0 0.0 copy-start.7
  0.0 3.1 %pack.1 = (bf16[64,512]{1,0:T(8,128)(2,1)}, bf16[64,512]{1,0:T(8,128)(2,1)}, bf16[8,256,512]{2,1,0:T(8,128)(2,1)}) custom-call(s32[1]{0:T(128)} %bitcast.1.core, bf16[256,512]{1,0:T(8,128)(2,1)} %tokens.1, bf16[32,128]{1,0:T(8,128)(2,1)} %bitcast.16, bf16[32,128]{1,0:T(8,128)(2,1)} %bitcast.17, bf16[32,128]{1,0:T(8,128)(2,1)} %fk.1, bf16[32,128]{1,0:T(8,128)(2,1)} %fv.1, ...), custom_call_target="tpu_custom_call" | custom-call | tf_op jit(solution)/shard_map/pack/pallas_call | solution.py:248
  3.1 0.0 copy-start.8
  3.1 0.0 copy-start.6
  3.1 4.7 %all-to-all-start = ((bf16[8,256,512]{2,1,0:T(8,128)(2,1)}), bf16[8,256,512]{2,1,0:T(8,128)(2,1)}, u32[]{:S(2)}, u32[]{:S(2)}) async-start(bf16[8,256,512]{2,1,0:T(8,128)(2,1)} %get-tuple-element.13), calls=%async_computation | async-start | bytes 4194304 | tf_op jit(solution)/shard_map/all_to_all | solution.py:273
  7.8 0.0 copy-start.2
  7.8 0.0 copy-start.3
  7.8 0.0 copy-start.4
  7.8 0.0 copy-done.8
  7.9 2.6 collective-permute-start
  10.4 0.1 pad_add_fusion.refs_0_
  10.5 0.8 collective-permute-done
  11.3 0.0 copy-done.7
  11.3 0.0 copy-done.6
  11.3 108.4 %all-gather.3 = f16[2048,512]{1,0:T(8,128)(2,1)S(1)} all-gather(f16[64,512]{1,0:T(8,128)(2,1)S(1)} %multiply_convert_fusion), channel_id=1, replica_groups=mesh['grp'=2,'sp_0'=32,'sp_1'=2,'tp'=4] {'sp_0'}, dimensions={0}, use_global_device_ids=true | all-gather | bytes 2162688 | tf_op jit(solution)/shard_map/all_gather | solution.py:281
  119.7 0.4 convert_convert_fusion.1
  120.1 0.0 all-to-all-done
  120.1 0.0 copy-done.2
  120.1 0.0 copy-done.3
  120.2 0.0 copy-done.4
  120.2 3.6 %project.1 = (bf16[512,128]{1,0:T(8,128)(2,1)S(1)}, bf16[512,64]{1,0:T(8,128)(2,1)S(1)}, bf16[512,32]{1,0:T(8,128)(2,1)S(1)}, bf16[512,32]{1,0:T(8,128)(2,1)S(1)}, f32[544,128]{1,0:T(8,128)S(1)}) custom-call(s32[2]{0:T(128)S(1)} %pad_add_fusion.refs_0_, f32[2]{0:T(128)S(1)} %copy-done.4, bf16[2048,512]{1,0:T(8,128)(2,1)} %bitcast.4.refs_2_, ...), custom_call_target="tpu_custom_call" | custom-call | tf_op jit(solution)/shard_map/project/pallas_call | solution.py:285
  123.8 82.0 %all-gather.4 = f16[17408,128]{1,0:T(8,128)(2,1)S(1)} all-gather(f16[544,128]{1,0:T(8,128)(2,1)S(1)} %convert_element_type.29), channel_id=2, replica_groups=mesh['grp'=2,'sp_0'=32,'sp_1'=2,'tp'=4] {'sp_0'}, dimensions={0}, use_global_device_ids=true | all-gather | bytes 4595712 | tf_op jit(solution)/shard_map/all_gather | solution.py:310
  205.8 0.0 copy-start
  205.8 0.0 copy-start.1
  205.8 0.0 copy-start.5
  205.8 0.5 convert_convert_fusion
  206.3 0.4 copy-done
  206.7 0.0 copy-done.1
  206.7 0.0 copy-done.5
  206.7 2.8 %shard_map.136 = bf16[512,128]{1,0:T(8,128)(2,1)} custom-call(s32[2]{0:T(128)S(1)} %pad_add_fusion.refs_0_, f32[2]{0:T(128)S(1)} %copy-done.4, bf16[512,128]{1,0:T(8,128)(2,1)S(1)} %get-tuple-element.16.refs_2_, bf16[512,64]{1,0:T(8,128)(2,1)S(1)} %get-tuple-element.17.refs_3_, bf16[512,32]{1,0:T(8,128)(2,1)S(1)} %get-tuple-element.18.refs_4_, ...), custom_call_target="tpu_custom_call" | custom-call | tf_op jit(solution)/shard_map/pallas_call | solution.py:313
  209.5 4.1 %all-to-all-start.1 = ((bf16[8,64,128]{2,1,0:T(8,128)(2,1)}), bf16[8,64,128]{2,1,0:T(8,128)(2,1)S(1)}, u32[]{:S(2)}, u32[]{:S(2)}) async-start(bf16[8,64,128]{2,1,0:T(8,128)(2,1)} %bitcast.10), calls=%async_computation.1 | async-start | bytes 262144 | tf_op jit(solution)/shard_map/all_to_all | solution.py:329
  213.6 0.1 slice.4
  213.7 5.5 %all-to-all-done.1.refs_0_ = bf16[8,64,128]{2,1,0:T(8,128)(2,1)S(1)} async-done(((bf16[8,64,128]{2,1,0:T(8,128)(2,1)}), bf16[8,64,128]{2,1,0:T(8,128)(2,1)S(1)}, u32[]{:S(2)}, u32[]{:S(2)}) %all-to-all-start.1) | async-done | bytes 131104 | tf_op jit(solution)/shard_map/all_to_all | solution.py:329
  219.2 0.5 broadcast_in_dim.10
  219.8 51.8 %all_to_all.15.refs_1_ = bf16[8,2048,128]{2,1,0:T(8,128)(2,1)S(1)} all-to-all(bf16[8,2048,128]{2,1,0:T(8,128)(2,1)S(1)} %broadcast_in_dim.10), channel_id=1, replica_groups=mesh['grp'=2,'sp_0'=32,'sp_1'=2,'tp'=4] {'sp_1','tp'}, dimensions={0} | all-to-all | bytes 8388608 | tf_op jit(solution)/shard_map/all_to_all | solution.py:308
  271.5 2.3 shard_map.137
  (2 shorter events, 0.1 us)
Async XLA Ops:
  0.0 11.3 %copy-start.7 = (f32[512]{0:T(512)S(1)}, f32[512]{0:T(512)}, u32[]{:S(2)}) copy-start(f32[512]{0:T(512)} %constant.15.clone.1) | copy-start | bytes 6148
  3.1 4.8 %copy-start.8 = (bf16[64,512]{1,0:T(8,128)(2,1)S(1)}, bf16[64,512]{1,0:T(8,128)(2,1)}, u32[]{:S(2)}) copy-start(bf16[64,512]{1,0:T(8,128)(2,1)} %get-tuple-element.15) | copy-start | bytes 196612
  3.1 8.2 %copy-start.6 = (bf16[64,512]{1,0:T(8,128)(2,1)S(1)}, bf16[64,512]{1,0:T(8,128)(2,1)}, u32[]{:S(2)}) copy-start(bf16[64,512]{1,0:T(8,128)(2,1)} %get-tuple-element.14) | copy-start | bytes 196612
  3.1 117.0 %all-to-all-start = ((bf16[8,256,512]{2,1,0:T(8,128)(2,1)}), bf16[8,256,512]{2,1,0:T(8,128)(2,1)}, u32[]{:S(2)}, u32[]{:S(2)}) async-start(bf16[8,256,512]{2,1,0:T(8,128)(2,1)} %get-tuple-element.13), calls=%async_computation | async-start | bytes 4194304 | tf_op jit(solution)/shard_map/all_to_all | solution.py:273
  7.8 112.3 %copy-start.2 = (f32[2048]{0:T(1024)S(1)}, f32[2048]{0:T(1024)}, u32[]{:S(2)}) copy-start(f32[2048]{0:T(1024)} %param.15) | copy-start | bytes 24580
  7.8 112.3 %copy-start.3 = (f32[1,512]{1,0:T(1,128)S(1)}, f32[1,512]{1,0:T(1,128)}, u32[]{:S(2)}) copy-start(f32[1,512]{1,0:T(1,128)} %constant.16.clone.1.refs_5_) | copy-start | bytes 6148
  7.8 112.3 %copy-start.4 = (f32[2]{0:T(128)S(1)}, f32[2]{0:T(128)}, u32[]{:S(2)}) copy-start(f32[2]{0:T(128)} %refs_1_.3) | copy-start | bytes 28
  7.9 3.4 %collective-permute-start = (bf16[64,512]{1,0:T(8,128)(2,1)S(1)}, bf16[64,512]{1,0:T(8,128)(2,1)S(1)}, u32[]{:S(2)}, u32[]{:S(2)}) collective-permute-start(bf16[64,512]{1,0:T(8,128)(2,1)S(1)} %copy-done.8), channel_id=1, source_target_pairs={{0,4},{4,0},{1,5},{5,1},{2,6},{6,2},{3,7},{7,3},{8,12},{12,8},{9,1... | collective-permute-start | bytes 196616 | tf_op jit(solution)/shard_map/ppermute | solution.py:275
  205.8 0.9 copy-start
  205.8 0.9 copy-start.1
  205.8 0.9 copy-start.5
  209.5 9.7 %all-to-all-start.1 = ((bf16[8,64,128]{2,1,0:T(8,128)(2,1)}), bf16[8,64,128]{2,1,0:T(8,128)(2,1)S(1)}, u32[]{:S(2)}, u32[]{:S(2)}) async-start(bf16[8,64,128]{2,1,0:T(8,128)(2,1)} %bitcast.10), calls=%async_computation.1 | async-start | bytes 262144 | tf_op jit(solution)/shard_map/all_to_all | solution.py:329

commit v5 on v4

--- a/solution.py
+++ b/solution.py
@@ -46,6 +46,13 @@
 def copies(source, target, signals):
     return [
         pltpu.make_async_copy(source, target.at[k], signals.at[k]) for k in range(target.shape[0])
+    ]
+
+
+def arrivals(source, target, signals):
+    return [
+        pltpu.make_async_copy(source.at[k], target.at[k], signals.at[k])
+        for k in range(target.shape[0])
     ]
 
 
@@ -80,7 +87,7 @@
 def project_kernel(
     place,
     decays,
-    tokens,
+    arrived,
     gains,
     weights,
     back,
@@ -89,26 +96,31 @@
     keys,
     queries,
     payload,
+    tokens,
+    signals,
     *,
     key,
     cores,
 ):
     f32, bf16 = jnp.float32, jnp.bfloat16
-    width = tokens.shape[1]
+    rows, width = tokens.shape[1:]
     parts, value = weights.shape[0], 2 * key
-    rows = tokens.shape[0] // (cores * parts)
+    arriving = arrivals(arrived, tokens, signals)
+    for copy in arriving:
+        copy.start()
     first, last = 2 * value, 6 * value + 2 * key
     factors = []
     for c in range(cores):
         square = jnp.zeros((rows, 1), f32)
         for k in range(parts):
-            x = tokens[(c * parts + k) * rows : (c * parts + k + 1) * rows, :].astype(f32)
+            arriving[c * parts + k].wait()
+            x = tokens[c * parts + k].astype(f32)
             square = square + jnp.sum(x * x, axis=1, keepdims=True)
         factors.append(lax.rsqrt(square * (1.0 / (parts * width)) + EPSILON))
     for c in range(cores):
         total = jnp.zeros((rows, last - first), f32)
         for k in range(parts):
-            x = tokens[(c * parts + k) * rows : (c * parts + k + 1) * rows, :].astype(f32)
+            x = tokens[c * parts + k].astype(f32)
             normed = (x * factors[c] * gains[k]).astype(bf16)
             total = total + dot(normed, weights[k][:, first:last])
         total = (total * back[:, first:last]).astype(bf16)
@@ -191,10 +203,16 @@
     mix[...] = jnp.concatenate(joined, axis=1).astype(bf16)
 
 
-def output_kernel(mixes, weights, out, *, cores):
+def output_kernel(mixes, stored, out, weights, signals, *, cores):
     parts = mixes.shape[0] // cores
+    arriving = arrivals(stored, weights, signals)
+    for k in range(parts):
+        for c in range(cores):
+            arriving[c * parts + k].start()
     summed = jnp.zeros(out.shape, jnp.float32)
     for k in range(parts):
+        for c in range(cores):
+            arriving[c * parts + k].wait()
         partial = sum(
             dot(mixes[c * parts + k], weights[c * parts + k], NT) for c in range(cores)
         )
@@ -291,14 +309,18 @@
             jax.ShapeDtypeStruct((chunk, key), bf16),
             jax.ShapeDtypeStruct((chunk + key, 2 * value), f32),
         ),
-        in_specs=[SMEM, SMEM] + [VMEM] * 4,
+        in_specs=[SMEM, SMEM, HBM, VMEM, VMEM, VMEM],
         out_specs=(VMEM,) * 5,
+        scratch_shapes=[
+            pltpu.VMEM(wide.shape, bf16),
+            pltpu.SemaphoreType.DMA((peers,)),
+        ],
         compiler_params=pltpu.CompilerParams(vmem_limit_bytes=20 * MIB),
         name="project",
     )(
         place,
         ret_decay,
-        wide.reshape(-1, width),
+        wide,
         norm_gain.reshape(tp, 1, width),
         weights.reshape(tp, width, padded),
         (1.0 / forth)[None],
@@ -327,11 +349,17 @@
 
     final = rows // tp
     mixes = lax.all_to_all(mix.reshape(cores * tp, final, -1), CHIP, 0, 0, tiled=True)
-    return kernel(
+    return pl.pallas_call(
         lambda *refs: output_kernel(*refs, cores=cores),
-        jax.ShapeDtypeStruct((final, out_weights.shape[1]), bf16),
-        [VMEM, VMEM],
-        16,
+        out_shape=jax.ShapeDtypeStruct((final, out_weights.shape[1]), bf16),
+        in_specs=[VMEM, HBM],
+        out_specs=VMEM,
+        scratch_shapes=[
+            pltpu.VMEM(out_weights.shape, bf16),
+            pltpu.SemaphoreType.DMA((peers,)),
+        ],
+        compiler_params=pltpu.CompilerParams(vmem_limit_bytes=16 * MIB),
+        name="output",
     )(mixes, out_weights)
 
 

time: 276 us -> 278 us (level)
  no operation moved by 1% of the time
where the time goes in v5:
time: 278 us; the launch traced here: 276 us
  blocking collectives  241 us (87%)
  starting transfers between devices  13.1 us (5%)
  Pallas kernels  13 us (5%)
  waiting for transfers between devices  6.31 us (2%)
    all_gather x1, blocking collectives, layer(): lax.all_gather((packed * forth).astype(f16), 'sp_0', axis=0, tiled=True)  108 us
    all_gather x1, blocking collectives, layer(): gathered = lax.all_gather(payload.astype(f16), 'sp_0', axis=0, tiled=False)  81.4 us
    all_to_all x1, blocking collectives, layer(): out_weights = lax.all_to_all(sent, CHIP, 0, 0, tiled=True)  51.8 us
    all_to_all x1, starting transfers between devices, layer(): lax.all_to_all(mix.reshape(cores * tp, final, -1), CHIP, 0, 0, tiled=True)  5.8 us
  transfers between devices with their start and end apart: 3, of which 2 were waited for; matrix products, arithmetic and copies ran while one was open for 0% of the time, Pallas kernels for 0%

profile of v5, /device:TPU:40, one launch (start us, length us, event | category | flops | bytes accessed | tf_op | source)
XLA Modules:
  0.0 275.7 jit_solution(7163367846308964368)
XLA Ops:
  0.0 0.0 copy-start.7
  0.0 3.1 %pack.1 = (bf16[64,512]{1,0:T(8,128)(2,1)}, bf16[64,512]{1,0:T(8,128)(2,1)}, bf16[8,256,512]{2,1,0:T(8,128)(2,1)}) custom-call(s32[1]{0:T(128)} %bitcast.1.core, bf16[256,512]{1,0:T(8,128)(2,1)} %tokens.1, bf16[32,128]{1,0:T(8,128)(2,1)} %bitcast.15, bf16[32,128]{1,0:T(8,128)(2,1)} %bitcast.16, bf16[32,128]{1,0:T(8,128)(2,1)} %fk.1, bf16[32,128]{1,0:T(8,128)(2,1)} %fv.1, ...), custom_call_target="tpu_custom_call" | custom-call | tf_op jit(solution)/shard_map/pack/pallas_call | solution.py:266
  3.1 0.0 copy-start.8
  3.1 0.0 copy-start.6
  3.1 4.7 %all-to-all-start = ((bf16[8,256,512]{2,1,0:T(8,128)(2,1)}), bf16[8,256,512]{2,1,0:T(8,128)(2,1)}, u32[]{:S(2)}, u32[]{:S(2)}) async-start(bf16[8,256,512]{2,1,0:T(8,128)(2,1)} %get-tuple-element.13), calls=%async_computation | async-start | bytes 4194304 | tf_op jit(solution)/shard_map/all_to_all | solution.py:291
  7.8 0.0 copy-start.2
  7.8 0.0 copy-start.3
  7.8 0.0 copy-start.4
  7.8 0.0 copy-done.8
  7.9 2.6 collective-permute-start
  10.4 0.1 pad_add_fusion.refs_0_
  10.5 0.8 collective-permute-done
  11.3 0.0 copy-done.7
  11.3 0.0 copy-done.6
  11.3 107.8 %all-gather.3 = f16[2048,512]{1,0:T(8,128)(2,1)S(1)} all-gather(f16[64,512]{1,0:T(8,128)(2,1)S(1)} %multiply_convert_fusion), channel_id=1, replica_groups=mesh['grp'=2,'sp_0'=32,'sp_1'=2,'tp'=4] {'sp_0'}, dimensions={0}, use_global_device_ids=true | all-gather | bytes 2162688 | tf_op jit(solution)/shard_map/all_gather | solution.py:299
  119.2 0.4 convert_convert_fusion.1
  119.6 0.0 all-to-all-done.refs_2_
  119.6 0.0 copy-done.2
  119.6 0.0 copy-done.3
  119.6 0.0 copy-done.4
  119.6 4.1 %project.1 = (bf16[512,128]{1,0:T(8,128)(2,1)S(1)}, bf16[512,64]{1,0:T(8,128)(2,1)S(1)}, bf16[512,32]{1,0:T(8,128)(2,1)S(1)}, bf16[512,32]{1,0:T(8,128)(2,1)S(1)}, f32[544,128]{1,0:T(8,128)S(1)}) custom-call(s32[2]{0:T(128)S(1)} %pad_add_fusion.refs_0_, f32[2]{0:T(128)S(1)} %copy-done.4, bf16[8,256,512]{2,1,0:T(8,128)(2,1)} %all-to-all-done.refs_2_, ...), custom_call_target="tpu_custom_call" | custom-call | tf_op jit(solution)/shard_map/project/pallas_call | solution.py:303
  123.8 81.4 %all-gather.4 = f16[17408,128]{1,0:T(8,128)(2,1)S(1)} all-gather(f16[544,128]{1,0:T(8,128)(2,1)S(1)} %convert_element_type.29), channel_id=2, replica_groups=mesh['grp'=2,'sp_0'=32,'sp_1'=2,'tp'=4] {'sp_0'}, dimensions={0}, use_global_device_ids=true | all-gather | bytes 4595712 | tf_op jit(solution)/shard_map/all_gather | solution.py:332
  205.2 0.0 copy-start
  205.2 0.0 copy-start.1
  205.2 0.0 copy-start.5
  205.2 0.5 convert_convert_fusion
  205.8 0.4 copy-done
  206.1 0.0 copy-done.1
  206.2 0.0 copy-done.5
  206.2 2.8 %shard_map.136 = bf16[512,128]{1,0:T(8,128)(2,1)} custom-call(s32[2]{0:T(128)S(1)} %pad_add_fusion.refs_0_, f32[2]{0:T(128)S(1)} %copy-done.4, bf16[512,128]{1,0:T(8,128)(2,1)S(1)} %get-tuple-element.16.refs_2_, bf16[512,64]{1,0:T(8,128)(2,1)S(1)} %get-tuple-element.17.refs_3_, bf16[512,32]{1,0:T(8,128)(2,1)S(1)} %get-tuple-element.18.refs_4_, ...), custom_call_target="tpu_custom_call" | custom-call | tf_op jit(solution)/shard_map/pallas_call | solution.py:335
  209.0 5.8 %all-to-all-start.1 = ((bf16[8,64,128]{2,1,0:T(8,128)(2,1)}), bf16[8,64,128]{2,1,0:T(8,128)(2,1)S(1)}, u32[]{:S(2)}, u32[]{:S(2)}) async-start(bf16[8,64,128]{2,1,0:T(8,128)(2,1)} %bitcast.9), calls=%async_computation.1 | async-start | bytes 262144 | tf_op jit(solution)/shard_map/all_to_all | solution.py:351
  214.8 0.1 slice.4
  214.9 5.5 %all-to-all-done.1.refs_0_ = bf16[8,64,128]{2,1,0:T(8,128)(2,1)S(1)} async-done(((bf16[8,64,128]{2,1,0:T(8,128)(2,1)}), bf16[8,64,128]{2,1,0:T(8,128)(2,1)S(1)}, u32[]{:S(2)}, u32[]{:S(2)}) %all-to-all-start.1) | async-done | bytes 131104 | tf_op jit(solution)/shard_map/all_to_all | solution.py:351
  220.4 0.5 broadcast_in_dim.10
  220.9 51.8 %all_to_all.15.refs_1_ = bf16[8,2048,128]{2,1,0:T(8,128)(2,1)S(1)} all-to-all(bf16[8,2048,128]{2,1,0:T(8,128)(2,1)S(1)} %broadcast_in_dim.10), channel_id=1, replica_groups=mesh['grp'=2,'sp_0'=32,'sp_1'=2,'tp'=4] {'sp_1','tp'}, dimensions={0} | all-to-all | bytes 8388608 | tf_op jit(solution)/shard_map/all_to_all | solution.py:330
  272.7 3.0 %output.1 = bf16[64,2048]{1,0:T(8,128)(2,1)} custom-call(bf16[8,64,128]{2,1,0:T(8,128)(2,1)S(1)} %all-to-all-done.1.refs_0_, bf16[8,2048,128]{2,1,0:T(8,128)(2,1)S(1)} %all_to_all.15.refs_1_), custom_call_target="tpu_custom_call" | custom-call | tf_op jit(solution)/shard_map/output/pallas_call | solution.py:352
  (2 shorter events, 0.1 us)
Async XLA Ops:
  0.0 11.3 %copy-start.7 = (f32[512]{0:T(512)S(1)}, f32[512]{0:T(512)}, u32[]{:S(2)}) copy-start(f32[512]{0:T(512)} %constant.15.clone.1) | copy-start | bytes 6148
  3.1 4.8 %copy-start.8 = (bf16[64,512]{1,0:T(8,128)(2,1)S(1)}, bf16[64,512]{1,0:T(8,128)(2,1)}, u32[]{:S(2)}) copy-start(bf16[64,512]{1,0:T(8,128)(2,1)} %get-tuple-element.15) | copy-start | bytes 196612
  3.1 8.2 %copy-start.6 = (bf16[64,512]{1,0:T(8,128)(2,1)S(1)}, bf16[64,512]{1,0:T(8,128)(2,1)}, u32[]{:S(2)}) copy-start(bf16[64,512]{1,0:T(8,128)(2,1)} %get-tuple-element.14) | copy-start | bytes 196612
  3.1 116.5 %all-to-all-start = ((bf16[8,256,512]{2,1,0:T(8,128)(2,1)}), bf16[8,256,512]{2,1,0:T(8,128)(2,1)}, u32[]{:S(2)}, u32[]{:S(2)}) async-start(bf16[8,256,512]{2,1,0:T(8,128)(2,1)} %get-tuple-element.13), calls=%async_computation | async-start | bytes 4194304 | tf_op jit(solution)/shard_map/all_to_all | solution.py:291
  7.8 111.8 %copy-start.2 = (f32[2048]{0:T(1024)S(1)}, f32[2048]{0:T(1024)}, u32[]{:S(2)}) copy-start(f32[2048]{0:T(1024)} %param.15) | copy-start | bytes 24580
  7.8 111.8 %copy-start.3 = (f32[1,512]{1,0:T(1,128)S(1)}, f32[1,512]{1,0:T(1,128)}, u32[]{:S(2)}) copy-start(f32[1,512]{1,0:T(1,128)} %constant.16.clone.1.refs_5_) | copy-start | bytes 6148
  7.8 111.8 %copy-start.4 = (f32[2]{0:T(128)S(1)}, f32[2]{0:T(128)}, u32[]{:S(2)}) copy-start(f32[2]{0:T(128)} %refs_1_.3) | copy-start | bytes 28
  7.9 3.4 %collective-permute-start = (bf16[64,512]{1,0:T(8,128)(2,1)S(1)}, bf16[64,512]{1,0:T(8,128)(2,1)S(1)}, u32[]{:S(2)}, u32[]{:S(2)}) collective-permute-start(bf16[64,512]{1,0:T(8,128)(2,1)S(1)} %copy-done.8), channel_id=1, source_target_pairs={{0,4},{4,0},{1,5},{5,1},{2,6},{6,2},{3,7},{7,3},{8,12},{12,8},{9,1... | collective-permute-start | bytes 196616 | tf_op jit(solution)/shard_map/ppermute | solution.py:293
  205.2 0.9 copy-start
  205.2 0.9 copy-start.1
  205.2 0.9 copy-start.5
  209.0 11.4 %all-to-all-start.1 = ((bf16[8,64,128]{2,1,0:T(8,128)(2,1)}), bf16[8,64,128]{2,1,0:T(8,128)(2,1)S(1)}, u32[]{:S(2)}, u32[]{:S(2)}) async-start(bf16[8,64,128]{2,1,0:T(8,128)(2,1)} %bitcast.9), calls=%async_computation.1 | async-start | bytes 262144 | tf_op jit(solution)/shard_map/all_to_all | solution.py:351

commit v6 on v5

--- a/solution.py
+++ b/solution.py
@@ -65,21 +65,35 @@
     for copy in started:
         copy.start()
 
-    def columns(ref, h):
+    def columns(ref, h, scale):
         size = ref.shape[1] // heads
-        return ref[...].astype(f32)[:, h * size : (h + 1) * size]
-
-    both = []
-    for h in range(heads):
-        parts = [columns(ref, h) for ref in (out_ret, out_fox, fk, fv, fq, rv, rk, rq)]
-        joined = jnp.concatenate(parts, axis=1)
-        blank = mine.shape[1] - joined.shape[1]
-        both.append(jnp.concatenate([joined, jnp.zeros((joined.shape[0], blank), f32)], axis=1))
-    shard = both[0].shape[0]
+        return ref[...].astype(f32)[:, h * size : (h + 1) * size] * scale
+
+    groups = (
+        ((out_ret, SMALL_WEIGHT), (out_fox, FOX_OUT_WEIGHT)),
+        ((fk, SMALL_WEIGHT), (fv, SMALL_WEIGHT)),
+        ((fq, QUERY_WEIGHT), (rv, SMALL_WEIGHT)),
+        ((rk, SMALL_WEIGHT), (rq, SMALL_WEIGHT)),
+    )
+    both = [
+        [jnp.concatenate([columns(ref, h, scale) for ref, scale in group], axis=1) for group in groups]
+        for h in range(heads)
+    ]
+    first = core[0] == 0
+    shard = both[0][0].shape[0]
     for c in range(heads):
-        at = slice(c * shard, (c + 1) * shard)
-        mine[at, :] = jnp.where(core[0] == c, both[c], 0.0).astype(mine.dtype)
-        theirs[at, :] = jnp.where(core[0] == c, both[1 - c], 0.0).astype(theirs.dtype)
+        for g in range(3):
+            at = slice((g * heads + c) * shard, (g * heads + c + 1) * shard)
+            mine[at, :] = jnp.where(core[0] == c, both[c][g], 0.0).astype(mine.dtype)
+            theirs[at, :] = jnp.where(core[0] == c, both[1 - c][g], 0.0).astype(theirs.dtype)
+    at = slice(3 * heads * shard, (3 * heads + 1) * shard)
+
+    def halves(left, right):
+        left, right = jnp.where(first, left, 0.0), jnp.where(first, 0.0, right)
+        return jnp.concatenate([left, right], axis=1)
+
+    mine[at, :] = halves(both[0][3], both[1][3]).astype(mine.dtype)
+    theirs[at, :] = halves(both[1][3], both[0][3]).astype(theirs.dtype)
     for copy in started:
         copy.wait()
 
@@ -87,51 +101,57 @@
 def project_kernel(
     place,
     decays,
-    arrived,
+    tokens,
     gains,
     weights,
-    back,
     query,
     values,
     keys,
     queries,
     payload,
-    tokens,
-    signals,
     *,
     key,
     cores,
 ):
     f32, bf16 = jnp.float32, jnp.bfloat16
-    rows, width = tokens.shape[1:]
-    parts, value = weights.shape[0], 2 * key
-    arriving = arrivals(arrived, tokens, signals)
-    for copy in arriving:
-        copy.start()
-    first, last = 2 * value, 6 * value + 2 * key
+    width = tokens.shape[1]
+    parts, value = gains.shape[0], 2 * key
+    rows = tokens.shape[0] // (cores * parts)
+    per = weights.shape[0] // parts
+    side = width // per
+    blocks = []
+    for k in range(parts):
+        at = slice(k * per, (k + 1) * per)
+        pair = weights[at, side : 2 * side, :].reshape(width, 2 * value)
+        mixed = weights[at, 2 * side : 3 * side, :].reshape(width, 2 * value)
+        last = weights[at, 3 * side :, :]
+        last = jnp.concatenate([last[:, :, :value], last[:, :, value:]], axis=1)
+        blocks.append((pair, mixed, last.reshape(width, value)))
     factors = []
     for c in range(cores):
         square = jnp.zeros((rows, 1), f32)
         for k in range(parts):
-            arriving[c * parts + k].wait()
-            x = tokens[c * parts + k].astype(f32)
+            x = tokens[(c * parts + k) * rows : (c * parts + k + 1) * rows, :].astype(f32)
             square = square + jnp.sum(x * x, axis=1, keepdims=True)
         factors.append(lax.rsqrt(square * (1.0 / (parts * width)) + EPSILON))
     for c in range(cores):
-        total = jnp.zeros((rows, last - first), f32)
+        sums = [jnp.zeros((rows, block.shape[1]), f32) for block in blocks[0]]
         for k in range(parts):
-            x = tokens[c * parts + k].astype(f32)
+            x = tokens[(c * parts + k) * rows : (c * parts + k + 1) * rows, :].astype(f32)
             normed = (x * factors[c] * gains[k]).astype(bf16)
-            total = total + dot(normed, weights[k][:, first:last])
-        total = (total * back[:, first:last]).astype(bf16)
+            sums = [total + dot(normed, block) for total, block in zip(sums, blocks[k])]
+        pair, mixed, last = sums
+        lane = lax.broadcasted_iota(jnp.int32, (rows, 2 * value), 1)
+        back = jnp.where(lane < value, 1.0 / QUERY_WEIGHT, 1.0 / SMALL_WEIGHT)
+        pair = (pair * (1.0 / SMALL_WEIGHT)).astype(bf16)
+        mixed = (mixed * back).astype(bf16)
+        last = (last * (1.0 / SMALL_WEIGHT)).astype(bf16)
         at = slice(c * rows, (c + 1) * rows)
-        payload[at, :] = total[:, : 2 * value].astype(f32) * KEY_VALUE
-        lane = lax.broadcasted_iota(jnp.int32, (rows, 2 * value), 1)
-        mixed = total[:, 2 * value : 4 * value].astype(f32)
-        query[at, :] = jnp.where(lane < value, mixed, 0.0).astype(bf16)
-        values[at, :] = total[:, 3 * value : 4 * value]
-        keys[at, :] = total[:, 4 * value : 4 * value + key]
-        queries[at, :] = total[:, 4 * value + key : 4 * value + 2 * key]
+        payload[at, :] = pair.astype(f32) * KEY_VALUE
+        query[at, :] = jnp.where(lane < value, mixed.astype(f32), 0.0).astype(bf16)
+        values[at, :] = mixed[:, value:]
+        keys[at, :] = last[:, :key]
+        queries[at, :] = last[:, key:]
     chunk = rows * cores
     trailing = jnp.exp((chunk - 1.0 - column_of(chunk)) * decays[place[1]]) * key ** (-0.5)
     high, low = two_terms(keys[...].astype(f32) * trailing)
@@ -260,14 +280,12 @@
 
     peers = cores * tp
     shard = fox_key_weight.shape[0]
-    chip_shard = shard * cores
-    lanes = 6 * value + 2 * key
-    padded = lanes + -lanes % 128
+    packed_rows = (3 * cores + 1) * shard
     mine, theirs, sent = pl.pallas_call(
         pack_kernel,
         out_shape=(
-            jax.ShapeDtypeStruct((chip_shard, padded), bf16),
-            jax.ShapeDtypeStruct((chip_shard, padded), bf16),
+            jax.ShapeDtypeStruct((packed_rows, 2 * value), bf16),
+            jax.ShapeDtypeStruct((packed_rows, 2 * value), bf16),
             jax.ShapeDtypeStruct((peers, rows, width), bf16),
         ),
         grid=(1,),
@@ -291,15 +309,9 @@
     wide = lax.all_to_all(sent, CHIP, 0, 0, tiled=True)
 
     got = lax.ppermute(theirs, "sp_1", [(0, 1), (1, 0)])
-    packed = mine.astype(f32) + got.astype(f32)
-    widths = (value, value, value, value, value, value, key, key, padded - lanes)
-    scales = (SMALL_WEIGHT, FOX_OUT_WEIGHT, SMALL_WEIGHT, SMALL_WEIGHT, QUERY_WEIGHT)
-    scales += (SMALL_WEIGHT, SMALL_WEIGHT, SMALL_WEIGHT, 1.0)
-    forth = jnp.concatenate([jnp.full((w,), s, f32) for w, s in zip(widths, scales)])
-    weights = lax.all_gather(
-        (packed * forth).astype(f16), "sp_0", axis=0, tiled=True
-    )
-    weights = weights.astype(f32).astype(bf16)
+    packed = (mine.astype(f32) + got.astype(f32)).astype(f16)
+    weights = lax.all_gather(packed, "sp_0", axis=0, tiled=True).astype(f32).astype(bf16)
+    weights = weights.reshape(-1, packed_rows, 2 * value)
     *parts, payload = pl.pallas_call(
         lambda *refs: project_kernel(*refs, key=key, cores=cores),
         out_shape=(
@@ -309,24 +321,20 @@
             jax.ShapeDtypeStruct((chunk, key), bf16),
             jax.ShapeDtypeStruct((chunk + key, 2 * value), f32),
         ),
-        in_specs=[SMEM, SMEM, HBM, VMEM, VMEM, VMEM],
+        in_specs=[SMEM, SMEM, VMEM, VMEM, VMEM],
         out_specs=(VMEM,) * 5,
-        scratch_shapes=[
-            pltpu.VMEM(wide.shape, bf16),
-            pltpu.SemaphoreType.DMA((peers,)),
-        ],
         compiler_params=pltpu.CompilerParams(vmem_limit_bytes=20 * MIB),
         name="project",
     )(
         place,
         ret_decay,
-        wide,
+        wide.reshape(-1, width),
         norm_gain.reshape(tp, 1, width),
-        weights.reshape(tp, width, padded),
-        (1.0 / forth)[None],
-    )
-
-    sent = jnp.broadcast_to(weights[None, :, : 2 * value], (peers, weights.shape[0], 2 * value))
+        weights,
+    )
+
+    out_rows = weights[:, : shard * cores, :].reshape(-1, 2 * value)
+    sent = jnp.broadcast_to(out_rows[None], (peers, *out_rows.shape))
     out_weights = lax.all_to_all(sent, CHIP, 0, 0, tiled=True)
 
     gathered = lax.all_gather(payload.astype(f16), "sp_0", axis=0, tiled=False)

time: 278 us -> 275 us (0.989)
  no operation moved by 1% of the time
where the time goes in v6:
time: 275 us; the launch traced here: 273 us
  blocking collectives  240 us (87%)
  Pallas kernels  13 us (5%)
  starting transfers between devices  11.4 us (4%)
  waiting for transfers between devices  6.31 us (2%)
    all_gather x1, blocking collectives, layer(): lax.all_gather(packed, 'sp_0', axis=0, tiled=True).astype(f32).astype(bf16)  107 us
    all_gather x1, blocking collectives, layer(): gathered = lax.all_gather(payload.astype(f16), 'sp_0', axis=0, tiled=False)  81.3 us
    all_to_all x1, blocking collectives, layer(): out_weights = lax.all_to_all(sent, CHIP, 0, 0, tiled=True)  51.8 us
    all_to_all x1, waiting for transfers between devices, layer(): lax.all_to_all(mix.reshape(cores * tp, final, -1), CHIP, 0, 0, tiled=True)  5.52 us
  transfers between devices with their start and end apart: 3, of which 2 were waited for; matrix products, arithmetic and copies ran while one was open for 0% of the time, Pallas kernels for 0%

profile of v6, /device:TPU:40, one launch (start us, length us, event | category | flops | bytes accessed | tf_op | source)
XLA Modules:
  0.0 273.0 jit_solution(16272575128391990247)
XLA Ops:
  0.0 3.0 %pack.1 = (bf16[224,128]{1,0:T(8,128)(2,1)}, bf16[224,128]{1,0:T(8,128)(2,1)}, bf16[8,256,512]{2,1,0:T(8,128)(2,1)}) custom-call(s32[1]{0:T(128)} %bitcast.1.core, bf16[256,512]{1,0:T(8,128)(2,1)} %tokens.1, bf16[32,128]{1,0:T(8,128)(2,1)} %bitcast.19, bf16[32,128]{1,0:T(8,128)(2,1)} %bitcast.20, bf16[32,128]{1,0:T(8,128)(2,1)} %fk.1, bf16[32,128]{1,0:T(8,128)(2,1)} %fv.1, ...), custom_call_target="tpu_custom_call" | custom-call | tf_op jit(solution)/shard_map/pack/pallas_call | solution.py:284
  3.0 0.0 copy-start.6
  3.1 0.0 copy-start.5
  3.1 0.0 copy-start.2
  3.1 0.0 copy-start.3
  3.1 4.7 %all-to-all-start = ((bf16[8,256,512]{2,1,0:T(8,128)(2,1)}), bf16[8,256,512]{2,1,0:T(8,128)(2,1)}, u32[]{:S(2)}, u32[]{:S(2)}) async-start(bf16[8,256,512]{2,1,0:T(8,128)(2,1)} %get-tuple-element.13), calls=%async_computation | async-start | bytes 4194304 | tf_op jit(solution)/shard_map/all_to_all | solution.py:309
  7.8 0.0 copy-done.6
  7.8 2.4 collective-permute-start
  10.3 0.1 pad_add_fusion.refs_0_
  10.3 0.8 collective-permute-done
  11.1 0.0 copy-done.5
  11.2 107.2 %all-gather.3 = f16[7168,128]{1,0:T(8,128)(2,1)S(1)} all-gather(f16[224,128]{1,0:T(8,128)(2,1)S(1)} %add_convert_fusion), channel_id=1, replica_groups=mesh['grp'=2,'sp_0'=32,'sp_1'=2,'tp'=4] {'sp_0'}, dimensions={0}, use_global_device_ids=true | all-gather | bytes 1892352 | tf_op jit(solution)/shard_map/all_gather | solution.py:313
  118.4 0.2 convert_convert_fusion.1
  118.6 0.0 all-to-all-done
  118.6 0.0 copy-done.2
  118.6 0.0 copy-done.3
  118.6 4.2 %project.1 = (bf16[512,128]{1,0:T(8,128)(2,1)S(1)}, bf16[512,64]{1,0:T(8,128)(2,1)S(1)}, bf16[512,32]{1,0:T(8,128)(2,1)S(1)}, bf16[512,32]{1,0:T(8,128)(2,1)S(1)}, f32[544,128]{1,0:T(8,128)S(1)}) custom-call(s32[2]{0:T(128)S(1)} %pad_add_fusion.refs_0_, f32[2]{0:T(128)S(1)} %copy-done.3, bf16[2048,512]{1,0:T(8,128)(2,1)} %bitcast.4.refs_2_, ...), custom_call_target="tpu_custom_call" | custom-call | tf_op jit(solution)/shard_map/project/pallas_call | solution.py:315
  122.8 81.3 %all-gather.4 = f16[17408,128]{1,0:T(8,128)(2,1)S(1)} all-gather(f16[544,128]{1,0:T(8,128)(2,1)S(1)} %convert_element_type.29), channel_id=2, replica_groups=mesh['grp'=2,'sp_0'=32,'sp_1'=2,'tp'=4] {'sp_0'}, dimensions={0}, use_global_device_ids=true | all-gather | bytes 4595712 | tf_op jit(solution)/shard_map/all_gather | solution.py:340
  204.1 0.0 copy-start
  204.1 0.0 copy-start.1
  204.1 0.0 copy-start.4
  204.1 0.5 convert_convert_fusion
  204.7 0.4 copy-done
  205.0 0.0 copy-done.1
  205.0 0.0 copy-done.4
  205.0 2.8 %shard_map.136 = bf16[512,128]{1,0:T(8,128)(2,1)} custom-call(s32[2]{0:T(128)S(1)} %pad_add_fusion.refs_0_, f32[2]{0:T(128)S(1)} %copy-done.3, bf16[512,128]{1,0:T(8,128)(2,1)S(1)} %get-tuple-element.16.refs_2_, bf16[512,64]{1,0:T(8,128)(2,1)S(1)} %get-tuple-element.17.refs_3_, bf16[512,32]{1,0:T(8,128)(2,1)S(1)} %get-tuple-element.18.refs_4_, ...), custom_call_target="tpu_custom_call" | custom-call | tf_op jit(solution)/shard_map/pallas_call | solution.py:343
  207.9 4.2 %all-to-all-start.1 = ((bf16[8,64,128]{2,1,0:T(8,128)(2,1)}), bf16[8,64,128]{2,1,0:T(8,128)(2,1)S(1)}, u32[]{:S(2)}, u32[]{:S(2)}) async-start(bf16[8,64,128]{2,1,0:T(8,128)(2,1)} %bitcast.10), calls=%async_computation.1 | async-start | bytes 262144 | tf_op jit(solution)/shard_map/all_to_all | solution.py:359
  212.1 0.1 slice.4
  212.1 5.5 %all-to-all-done.1.refs_0_ = bf16[8,64,128]{2,1,0:T(8,128)(2,1)S(1)} async-done(((bf16[8,64,128]{2,1,0:T(8,128)(2,1)}), bf16[8,64,128]{2,1,0:T(8,128)(2,1)S(1)}, u32[]{:S(2)}, u32[]{:S(2)}) %all-to-all-start.1) | async-done | bytes 131104 | tf_op jit(solution)/shard_map/all_to_all | solution.py:359
  217.6 0.5 broadcast_in_dim.12
  218.2 51.8 %all_to_all.15.refs_1_ = bf16[8,2048,128]{2,1,0:T(8,128)(2,1)S(1)} all-to-all(bf16[8,2048,128]{2,1,0:T(8,128)(2,1)S(1)} %broadcast_in_dim.12), channel_id=1, replica_groups=mesh['grp'=2,'sp_0'=32,'sp_1'=2,'tp'=4] {'sp_1','tp'}, dimensions={0} | all-to-all | bytes 8388608 | tf_op jit(solution)/shard_map/all_to_all | solution.py:338
  270.0 3.0 %output.1 = bf16[64,2048]{1,0:T(8,128)(2,1)} custom-call(bf16[8,64,128]{2,1,0:T(8,128)(2,1)S(1)} %all-to-all-done.1.refs_0_, bf16[8,2048,128]{2,1,0:T(8,128)(2,1)S(1)} %all_to_all.15.refs_1_), custom_call_target="tpu_custom_call" | custom-call | tf_op jit(solution)/shard_map/output/pallas_call | solution.py:360
  (2 shorter events, 0.1 us)
Async XLA Ops:
  3.0 4.8 %copy-start.6 = (bf16[224,128]{1,0:T(8,128)(2,1)S(1)}, bf16[224,128]{1,0:T(8,128)(2,1)}, u32[]{:S(2)}) copy-start(bf16[224,128]{1,0:T(8,128)(2,1)} %get-tuple-element.15) | copy-start | bytes 172036
  3.1 8.1 %copy-start.5 = (bf16[224,128]{1,0:T(8,128)(2,1)S(1)}, bf16[224,128]{1,0:T(8,128)(2,1)}, u32[]{:S(2)}) copy-start(bf16[224,128]{1,0:T(8,128)(2,1)} %get-tuple-element.14) | copy-start | bytes 172036
  3.1 115.5 %copy-start.2 = (f32[2048]{0:T(1024)S(1)}, f32[2048]{0:T(1024)}, u32[]{:S(2)}) copy-start(f32[2048]{0:T(1024)} %param.15) | copy-start | bytes 24580
  3.1 115.5 %copy-start.3 = (f32[2]{0:T(128)S(1)}, f32[2]{0:T(128)}, u32[]{:S(2)}) copy-start(f32[2]{0:T(128)} %refs_1_.3) | copy-start | bytes 28
  3.1 115.5 %all-to-all-start = ((bf16[8,256,512]{2,1,0:T(8,128)(2,1)}), bf16[8,256,512]{2,1,0:T(8,128)(2,1)}, u32[]{:S(2)}, u32[]{:S(2)}) async-start(bf16[8,256,512]{2,1,0:T(8,128)(2,1)} %get-tuple-element.13), calls=%async_computation | async-start | bytes 4194304 | tf_op jit(solution)/shard_map/all_to_all | solution.py:309
  7.8 3.3 %collective-permute-start = (bf16[224,128]{1,0:T(8,128)(2,1)S(1)}, bf16[224,128]{1,0:T(8,128)(2,1)S(1)}, u32[]{:S(2)}, u32[]{:S(2)}) collective-permute-start(bf16[224,128]{1,0:T(8,128)(2,1)S(1)} %copy-done.6), channel_id=1, source_target_pairs={{0,4},{4,0},{1,5},{5,1},{2,6},{6,2},{3,7},{7,3},{8,12},{12,8},{9,1... | collective-permute-start | bytes 172040 | tf_op jit(solution)/shard_map/ppermute | solution.py:311
  204.1 0.9 copy-start
  204.1 0.9 copy-start.1
  204.1 0.9 copy-start.4
  207.9 9.8 %all-to-all-start.1 = ((bf16[8,64,128]{2,1,0:T(8,128)(2,1)}), bf16[8,64,128]{2,1,0:T(8,128)(2,1)S(1)}, u32[]{:S(2)}, u32[]{:S(2)}) async-start(bf16[8,64,128]{2,1,0:T(8,128)(2,1)} %bitcast.10), calls=%async_computation.1 | async-start | bytes 262144 | tf_op jit(solution)/shard_map/all_to_all | solution.py:359

commit v7 on v6

--- a/solution.py
+++ b/solution.py
@@ -101,7 +101,7 @@
 def project_kernel(
     place,
     decays,
-    tokens,
+    arrived,
     gains,
     weights,
     query,
@@ -109,14 +109,18 @@
     keys,
     queries,
     payload,
+    tokens,
+    signals,
     *,
     key,
     cores,
 ):
     f32, bf16 = jnp.float32, jnp.bfloat16
-    width = tokens.shape[1]
+    rows, width = tokens.shape[1:]
     parts, value = gains.shape[0], 2 * key
-    rows = tokens.shape[0] // (cores * parts)
+    arriving = arrivals(arrived, tokens, signals)
+    for copy in arriving:
+        copy.start()
     per = weights.shape[0] // parts
     side = width // per
     blocks = []
@@ -131,13 +135,14 @@
     for c in range(cores):
         square = jnp.zeros((rows, 1), f32)
         for k in range(parts):
-            x = tokens[(c * parts + k) * rows : (c * parts + k + 1) * rows, :].astype(f32)
+            arriving[c * parts + k].wait()
+            x = tokens[c * parts + k].astype(f32)
             square = square + jnp.sum(x * x, axis=1, keepdims=True)
         factors.append(lax.rsqrt(square * (1.0 / (parts * width)) + EPSILON))
     for c in range(cores):
         sums = [jnp.zeros((rows, block.shape[1]), f32) for block in blocks[0]]
         for k in range(parts):
-            x = tokens[(c * parts + k) * rows : (c * parts + k + 1) * rows, :].astype(f32)
+            x = tokens[c * parts + k].astype(f32)
             normed = (x * factors[c] * gains[k]).astype(bf16)
             sums = [total + dot(normed, block) for total, block in zip(sums, blocks[k])]
         pair, mixed, last = sums
@@ -321,14 +326,18 @@
             jax.ShapeDtypeStruct((chunk, key), bf16),
             jax.ShapeDtypeStruct((chunk + key, 2 * value), f32),
         ),
-        in_specs=[SMEM, SMEM, VMEM, VMEM, VMEM],
+        in_specs=[SMEM, SMEM, HBM, VMEM, VMEM],
         out_specs=(VMEM,) * 5,
+        scratch_shapes=[
+            pltpu.VMEM(wide.shape, bf16),
+            pltpu.SemaphoreType.DMA((peers,)),
+        ],
         compiler_params=pltpu.CompilerParams(vmem_limit_bytes=20 * MIB),
         name="project",
     )(
         place,
         ret_decay,
-        wide.reshape(-1, width),
+        wide,
         norm_gain.reshape(tp, 1, width),
         weights,
     )

time: 275 us -> 275 us (level)
  no operation moved by 1% of the time
where the time goes in v7:
time: 275 us; the launch traced here: 273 us
  blocking collectives  240 us (87%)
  Pallas kernels  13.5 us (5%)
  starting transfers between devices  11.4 us (4%)
  waiting for transfers between devices  6.31 us (2%)
    all_gather x1, blocking collectives, layer(): lax.all_gather(packed, 'sp_0', axis=0, tiled=True).astype(f32).astype(bf16)  107 us
    all_gather x1, blocking collectives, layer(): gathered = lax.all_gather(payload.astype(f16), 'sp_0', axis=0, tiled=False)  81.8 us
    all_to_all x1, blocking collectives, layer(): out_weights = lax.all_to_all(sent, CHIP, 0, 0, tiled=True)  51.8 us
    all_to_all x1, waiting for transfers between devices, layer(): lax.all_to_all(mix.reshape(cores * tp, final, -1), CHIP, 0, 0, tiled=True)  5.52 us
  transfers between devices with their start and end apart: 3, of which 2 were waited for; matrix products, arithmetic and copies ran while one was open for 0% of the time, Pallas kernels for 0%

profile of v7, /device:TPU:40, one launch (start us, length us, event | category | flops | bytes accessed | tf_op | source)
XLA Modules:
  0.0 273.5 jit_solution(17759184014790122077)
XLA Ops:
  0.0 3.0 %pack.1 = (bf16[224,128]{1,0:T(8,128)(2,1)}, bf16[224,128]{1,0:T(8,128)(2,1)}, bf16[8,256,512]{2,1,0:T(8,128)(2,1)}) custom-call(s32[1]{0:T(128)} %bitcast.1.core, bf16[256,512]{1,0:T(8,128)(2,1)} %tokens.1, bf16[32,128]{1,0:T(8,128)(2,1)} %bitcast.18, bf16[32,128]{1,0:T(8,128)(2,1)} %bitcast.19, bf16[32,128]{1,0:T(8,128)(2,1)} %fk.1, bf16[32,128]{1,0:T(8,128)(2,1)} %fv.1, ...), custom_call_target="tpu_custom_call" | custom-call | tf_op jit(solution)/shard_map/pack/pallas_call | solution.py:289
  3.0 0.0 copy-start.6
  3.1 0.0 copy-start.5
  3.1 0.0 copy-start.2
  3.1 0.0 copy-start.3
  3.1 4.7 %all-to-all-start = ((bf16[8,256,512]{2,1,0:T(8,128)(2,1)}), bf16[8,256,512]{2,1,0:T(8,128)(2,1)}, u32[]{:S(2)}, u32[]{:S(2)}) async-start(bf16[8,256,512]{2,1,0:T(8,128)(2,1)} %get-tuple-element.13), calls=%async_computation | async-start | bytes 4194304 | tf_op jit(solution)/shard_map/all_to_all | solution.py:314
  7.8 0.0 copy-done.6
  7.8 2.4 collective-permute-start
  10.3 0.1 pad_add_fusion.refs_0_
  10.3 0.8 collective-permute-done
  11.1 0.0 copy-done.5
  11.2 106.7 %all-gather.3 = f16[7168,128]{1,0:T(8,128)(2,1)S(1)} all-gather(f16[224,128]{1,0:T(8,128)(2,1)S(1)} %add_convert_fusion), channel_id=1, replica_groups=mesh['grp'=2,'sp_0'=32,'sp_1'=2,'tp'=4] {'sp_0'}, dimensions={0}, use_global_device_ids=true | all-gather | bytes 1892352 | tf_op jit(solution)/shard_map/all_gather | solution.py:318
  117.9 0.2 convert_convert_fusion.1
  118.1 0.0 all-to-all-done.refs_2_
  118.1 0.0 copy-done.2
  118.1 0.0 copy-done.3
  118.1 4.6 %project.1 = (bf16[512,128]{1,0:T(8,128)(2,1)S(1)}, bf16[512,64]{1,0:T(8,128)(2,1)S(1)}, bf16[512,32]{1,0:T(8,128)(2,1)S(1)}, bf16[512,32]{1,0:T(8,128)(2,1)S(1)}, f32[544,128]{1,0:T(8,128)S(1)}) custom-call(s32[2]{0:T(128)S(1)} %pad_add_fusion.refs_0_, f32[2]{0:T(128)S(1)} %copy-done.3, bf16[8,256,512]{2,1,0:T(8,128)(2,1)} %all-to-all-done.refs_2_, ...), custom_call_target="tpu_custom_call" | custom-call | tf_op jit(solution)/shard_map/project/pallas_call | solution.py:320
  122.8 81.8 %all-gather.4 = f16[17408,128]{1,0:T(8,128)(2,1)S(1)} all-gather(f16[544,128]{1,0:T(8,128)(2,1)S(1)} %convert_element_type.29), channel_id=2, replica_groups=mesh['grp'=2,'sp_0'=32,'sp_1'=2,'tp'=4] {'sp_0'}, dimensions={0}, use_global_device_ids=true | all-gather | bytes 4595712 | tf_op jit(solution)/shard_map/all_gather | solution.py:349
  204.6 0.0 copy-start
  204.6 0.0 copy-start.1
  204.6 0.0 copy-start.4
  204.6 0.5 convert_convert_fusion
  205.1 0.4 copy-done
  205.5 0.0 copy-done.1
  205.5 0.0 copy-done.4
  205.5 2.8 %shard_map.136 = bf16[512,128]{1,0:T(8,128)(2,1)} custom-call(s32[2]{0:T(128)S(1)} %pad_add_fusion.refs_0_, f32[2]{0:T(128)S(1)} %copy-done.3, bf16[512,128]{1,0:T(8,128)(2,1)S(1)} %get-tuple-element.16.refs_2_, bf16[512,64]{1,0:T(8,128)(2,1)S(1)} %get-tuple-element.17.refs_3_, bf16[512,32]{1,0:T(8,128)(2,1)S(1)} %get-tuple-element.18.refs_4_, ...), custom_call_target="tpu_custom_call" | custom-call | tf_op jit(solution)/shard_map/pallas_call | solution.py:352
  208.3 4.3 %all-to-all-start.1 = ((bf16[8,64,128]{2,1,0:T(8,128)(2,1)}), bf16[8,64,128]{2,1,0:T(8,128)(2,1)S(1)}, u32[]{:S(2)}, u32[]{:S(2)}) async-start(bf16[8,64,128]{2,1,0:T(8,128)(2,1)} %bitcast.9), calls=%async_computation.1 | async-start | bytes 262144 | tf_op jit(solution)/shard_map/all_to_all | solution.py:368
  212.6 0.1 slice.4
  212.6 5.5 %all-to-all-done.1.refs_0_ = bf16[8,64,128]{2,1,0:T(8,128)(2,1)S(1)} async-done(((bf16[8,64,128]{2,1,0:T(8,128)(2,1)}), bf16[8,64,128]{2,1,0:T(8,128)(2,1)S(1)}, u32[]{:S(2)}, u32[]{:S(2)}) %all-to-all-start.1) | async-done | bytes 131104 | tf_op jit(solution)/shard_map/all_to_all | solution.py:368
  218.1 0.5 broadcast_in_dim.12
  218.7 51.8 %all_to_all.15.refs_1_ = bf16[8,2048,128]{2,1,0:T(8,128)(2,1)S(1)} all-to-all(bf16[8,2048,128]{2,1,0:T(8,128)(2,1)S(1)} %broadcast_in_dim.12), channel_id=1, replica_groups=mesh['grp'=2,'sp_0'=32,'sp_1'=2,'tp'=4] {'sp_1','tp'}, dimensions={0} | all-to-all | bytes 8388608 | tf_op jit(solution)/shard_map/all_to_all | solution.py:347
  270.5 3.0 %output.1 = bf16[64,2048]{1,0:T(8,128)(2,1)} custom-call(bf16[8,64,128]{2,1,0:T(8,128)(2,1)S(1)} %all-to-all-done.1.refs_0_, bf16[8,2048,128]{2,1,0:T(8,128)(2,1)S(1)} %all_to_all.15.refs_1_), custom_call_target="tpu_custom_call" | custom-call | tf_op jit(solution)/shard_map/output/pallas_call | solution.py:369
  (2 shorter events, 0.0 us)
Async XLA Ops:
  3.0 4.8 %copy-start.6 = (bf16[224,128]{1,0:T(8,128)(2,1)S(1)}, bf16[224,128]{1,0:T(8,128)(2,1)}, u32[]{:S(2)}) copy-start(bf16[224,128]{1,0:T(8,128)(2,1)} %get-tuple-element.15) | copy-start | bytes 172036
  3.1 8.1 %copy-start.5 = (bf16[224,128]{1,0:T(8,128)(2,1)S(1)}, bf16[224,128]{1,0:T(8,128)(2,1)}, u32[]{:S(2)}) copy-start(bf16[224,128]{1,0:T(8,128)(2,1)} %get-tuple-element.14) | copy-start | bytes 172036
  3.1 115.0 %copy-start.2 = (f32[2048]{0:T(1024)S(1)}, f32[2048]{0:T(1024)}, u32[]{:S(2)}) copy-start(f32[2048]{0:T(1024)} %param.15) | copy-start | bytes 24580
  3.1 115.0 %copy-start.3 = (f32[2]{0:T(128)S(1)}, f32[2]{0:T(128)}, u32[]{:S(2)}) copy-start(f32[2]{0:T(128)} %refs_1_.3) | copy-start | bytes 28
  3.1 115.0 %all-to-all-start = ((bf16[8,256,512]{2,1,0:T(8,128)(2,1)}), bf16[8,256,512]{2,1,0:T(8,128)(2,1)}, u32[]{:S(2)}, u32[]{:S(2)}) async-start(bf16[8,256,512]{2,1,0:T(8,128)(2,1)} %get-tuple-element.13), calls=%async_computation | async-start | bytes 4194304 | tf_op jit(solution)/shard_map/all_to_all | solution.py:314
  7.8 3.3 %collective-permute-start = (bf16[224,128]{1,0:T(8,128)(2,1)S(1)}, bf16[224,128]{1,0:T(8,128)(2,1)S(1)}, u32[]{:S(2)}, u32[]{:S(2)}) collective-permute-start(bf16[224,128]{1,0:T(8,128)(2,1)S(1)} %copy-done.6), channel_id=1, source_target_pairs={{0,4},{4,0},{1,5},{5,1},{2,6},{6,2},{3,7},{7,3},{8,12},{12,8},{9,1... | collective-permute-start | bytes 172040 | tf_op jit(solution)/shard_map/ppermute | solution.py:316
  204.6 0.9 copy-start
  204.6 0.9 copy-start.1
  204.6 0.9 copy-start.4
  208.3 9.8 %all-to-all-start.1 = ((bf16[8,64,128]{2,1,0:T(8,128)(2,1)}), bf16[8,64,128]{2,1,0:T(8,128)(2,1)S(1)}, u32[]{:S(2)}, u32[]{:S(2)}) async-start(bf16[8,64,128]{2,1,0:T(8,128)(2,1)} %bitcast.9), calls=%async_computation.1 | async-start | bytes 262144 | tf_op jit(solution)/shard_map/all_to_all | solution.py:368
